TPU v7x, 32 devices: a whole 2x2x4 slice. The times are simulated.
32 devices in a mesh: sp: 8 (over z, y), tp: 4 (over x, core).
Axes of the slice: x: 2, y: 2, z: 4, core: 2. Of those that a mesh axis runs over, the one named last changes fastest.
Arguments:
- tokens: bfloat16 [4096, 2048], P('sp', 'tp'), may hold values from -6 to 6
- norm_gain: float32 [2048], replicated, may hold values from 0.1 to 1.9
- query_weight: bfloat16 [2048, 2048], P('sp', 'tp'), may hold values from -0.125 to 0.125
- key_weight: bfloat16 [2048, 512], P('sp', 'tp'), may hold values from -0.125 to 0.125
- value_weight: bfloat16 [2048, 512], P('sp', 'tp'), may hold values from -0.125 to 0.125
- pool_in_weight: bfloat16 [2048, 1024], P('sp', 'tp'), may hold values from -0.125 to 0.125
- pool_mix_weight: bfloat16 [4, 256, 256], P('tp'), may hold values from -0.375 to 0.375
- sink_logit: float32 [32], P('tp'), may hold values from -300 to 300
- out_pool_weight: bfloat16 [1024, 2048], P('tp', 'sp'), may hold values from -0.109375 to 0.109375
- out_attn_weight: bfloat16 [2048, 2048], P('tp', 'sp'), may hold values from -1.25 to 1.25
Outputs:
- mixed: bfloat16 [4096, 2048], P('sp', 'tp')
- log_weight: float32 [32, 4096], P('tp', 'sp')
All inputs are finite; a program needn't handle non-finite values.
Results may differ from a plain program's by a relative error of at most 0.012.
Values may be sent and summed in bfloat16 or wider, within the bound.
No kernel may reach another device: no remote copies, remote signals or barrier semaphores. Data moves between devices by JAX's collectives and lax.ppermute only.
A program may use at most 64 MiB of HBM per device.

v0:
```python
import jax
import jax.numpy as jnp
from jax import lax
from jax.sharding import PartitionSpec as P

HD = 64
WINDOW = 128
GRID_W = 64


norm_eps = 1e-06
rope_base = 10000.0
pool_reach = 8
neg_fill = -1e30


def with_halo(cells, sides, width):
    for axis, dim in sides:
        count = lax.axis_size(axis)
        ends = count - 1
        head = lax.slice_in_dim(cells, 0, width, axis=dim)
        tail = lax.slice_in_dim(cells, cells.shape[dim] - width, cells.shape[dim], axis=dim)
        cells = jnp.concatenate(
            [
                lax.ppermute(tail, axis, [(i, (i + 1) % count) for i in range(ends)]),
                cells,
                lax.ppermute(head, axis, [((i + 1) % count, i) for i in range(ends)]),
            ],
            axis=dim,
        )
    return cells


def rope_tables(positions, head_dim):
    n_freq = head_dim // 4
    freqs = rope_base ** (-jnp.arange(n_freq, dtype=jnp.float32) / n_freq)
    rows = (positions // GRID_W).astype(jnp.float32)
    columns = (positions % GRID_W).astype(jnp.float32)
    row_angle = rows[:, None] * freqs[None, :]
    col_angle = columns[:, None] * freqs[None, :]
    return (jnp.cos(row_angle), jnp.sin(row_angle), jnp.cos(col_angle), jnp.sin(col_angle))


def rotate_half(values, cosine, sine):
    middle = values.shape[-1] // 2
    first = values[..., :middle]
    second = values[..., middle:]
    return jnp.concatenate([first * cosine - second * sine, second * cosine + first * sine], -1)


def rotate_heads(values, tables, head_dim):
    rows_count = values.shape[0]
    shaped = values.astype(jnp.float32).reshape(rows_count, -1, head_dim)
    cos_r, sin_r, cos_c, sin_c = [table[:, None, :] for table in tables]
    split = head_dim // 2
    turned = jnp.concatenate(
        [
            rotate_half(shaped[..., :split], cos_r, sin_r),
            rotate_half(shaped[..., split:], cos_c, sin_c),
        ],
        -1,
    )
    return turned.reshape(rows_count, -1).astype(jnp.bfloat16)


def pool_group(extended, own, positions, half_width, seq_total):
    rows_count = own.shape[0]
    summed = jnp.zeros(own.shape, jnp.float32)
    counted = jnp.zeros((rows_count,), jnp.float32)
    for shift_by in range(-pool_reach, pool_reach):
        source = positions + shift_by
        inside = (
            (shift_by >= -half_width)
            & (shift_by < half_width)
            & (source >= 0)
            & (source < seq_total)
        )
        window_rows = extended[pool_reach + shift_by : pool_reach + shift_by + rows_count].astype(
            jnp.float32
        )
        summed = summed + jnp.where(inside[:, None], window_rows, 0.0)
        counted = counted + inside.astype(jnp.float32)
    return (summed / counted[:, None] - own.astype(jnp.float32)).astype(jnp.bfloat16)


def attend_block(queries, keys, values, sink, query_pos, key_pos, seq_total):
    scores = jnp.einsum(
        "qhgd,khd->hgqk", queries, keys, preferred_element_type=jnp.float32
    ) * HD ** (-0.5)
    valid = (
        (jnp.abs(query_pos[:, None] - key_pos[None, :]) <= WINDOW)
        & (key_pos >= 0)[None, :]
        & (key_pos < seq_total)[None, :]
    )
    scores = jnp.where(valid, scores, neg_fill)
    row_top = jnp.maximum(jnp.max(scores, -1), sink[:, :, None])
    exps = jnp.exp(scores - row_top[..., None])
    row_total = jnp.sum(exps, -1) + jnp.exp(sink[:, :, None] - row_top)
    weights = (exps / row_total[..., None]).astype(jnp.bfloat16)
    attended = jnp.einsum("hgqk,khd->qhgd", weights, values, preferred_element_type=jnp.float32)
    return (attended.astype(jnp.bfloat16), row_top + jnp.log(row_total))


def fetch_outputs(out_pool_weight, out_attn_weight):
    return (
        lax.all_gather(out_pool_weight, "sp", axis=1, tiled=True),
        lax.all_gather(out_attn_weight, "sp", axis=1, tiled=True),
    )


def local(
    tokens,
    norm_gain,
    query_weight,
    key_weight,
    value_weight,
    pool_in_weight,
    pool_mix_weight,
    sink_logit,
    out_pool_weight,
    out_attn_weight,
):
    whole = lax.all_gather(tokens, "tp", axis=1, tiled=True)
    wide = whole.astype(jnp.float32)
    normed = (
        wide * lax.rsqrt(jnp.mean(wide * wide, -1, keepdims=True) + norm_eps) * norm_gain
    ).astype(jnp.bfloat16)
    tok_rows = normed.shape[0]
    seq_total = tok_rows * lax.axis_size("sp")
    offset = lax.axis_index("sp") * tok_rows
    weights_in = (query_weight, key_weight, value_weight, pool_in_weight)
    pieces = (
        lax.all_gather(weights_in[0], "sp", axis=0, tiled=True),
        lax.all_gather(weights_in[1], "sp", axis=0, tiled=True),
        lax.all_gather(weights_in[2], "sp", axis=0, tiled=True),
        lax.all_gather(weights_in[3], "sp", axis=0, tiled=True),
    )
    sums = tuple((jnp.dot(normed, piece, preferred_element_type=jnp.float32) for piece in pieces))
    query, key, value, pool_input = [total.astype(jnp.bfloat16) for total in sums]
    positions = offset + jnp.arange(tok_rows, dtype=jnp.int32)
    tables = rope_tables(positions, HD)
    rot_query = rotate_heads(query, tables, HD)
    rot_key = rotate_heads(key, tables, HD)
    key_width = rot_key.shape[1]
    pool_ext = with_halo(pool_input, (("sp", 0),), pool_reach)
    pair_ext = with_halo(jnp.concatenate([rot_key, value], 1), (("sp", 0),), WINDOW)
    key_ext = pair_ext[:, :key_width]
    value_ext = pair_ext[:, key_width:]
    half_width = jnp.left_shift(jnp.int32(1), lax.axis_index("tp"))
    pooled = pool_group(pool_ext, pool_input, positions, half_width, seq_total)
    pool_out = jnp.dot(pooled, pool_mix_weight[0], preferred_element_type=jnp.float32).astype(
        jnp.bfloat16
    )
    heads_local = rot_query.shape[1] // HD
    kv_local = key_width // HD
    grp = heads_local // kv_local
    query_heads = rot_query.reshape(tok_rows, kv_local, grp, HD)
    key_heads = key_ext.reshape(-1, kv_local, HD)
    value_heads = value_ext.reshape(-1, kv_local, HD)
    sink = sink_logit.reshape(kv_local, grp)
    block_rows = min(tok_rows, 256)
    attended_parts = []
    log_parts = []
    for block_index in range(tok_rows // block_rows):
        start = block_index * block_rows
        query_pos = offset + start + jnp.arange(block_rows, dtype=jnp.int32)
        key_pos = offset + start - WINDOW + jnp.arange(block_rows + 2 * WINDOW, dtype=jnp.int32)
        attended_block, log_block = attend_block(
            query_heads[start : start + block_rows],
            key_heads[start : start + block_rows + 2 * WINDOW],
            value_heads[start : start + block_rows + 2 * WINDOW],
            sink,
            query_pos,
            key_pos,
            seq_total,
        )
        attended_parts.append(attended_block.reshape(block_rows, heads_local * HD))
        log_parts.append(log_block.reshape(heads_local, block_rows))
    attended = jnp.concatenate(attended_parts, 0)
    log_weight = jnp.concatenate(log_parts, 1)
    out_pool_full, out_attn_full = fetch_outputs(out_pool_weight, out_attn_weight)
    term = jnp.dot(pool_out, out_pool_full, preferred_element_type=jnp.float32)
    term = term + jnp.dot(attended, out_attn_full, preferred_element_type=jnp.float32)
    mixed = lax.psum_scatter(term.astype(jnp.bfloat16), "tp", scatter_dimension=1, tiled=True)
    return (mixed, log_weight)


def solution(mesh):
    return jax.shard_map(
        local,
        mesh=mesh,
        in_specs=(
            P("sp", "tp"),
            P(),
            P("sp", "tp"),
            P("sp", "tp"),
            P("sp", "tp"),
            P("sp", "tp"),
            P("tp", None, None),
            P("tp"),
            P("tp", "sp"),
            P("tp", "sp"),
        ),
        out_specs=(P("sp", "tp"), P("tp", "sp")),
        check_vma=False,
    )
```

profile of v0, /device:TPU:0, one launch (start us, length us, event | category | flops | bytes accessed | tf_op | source)
XLA Modules:
  0.0 262.9 jit_solution(8358394788098384605)
XLA Ops:
  7.2 0.7 all-gather.6.cloned.1.call-update
  8.0 0.7 all-gather.8.cloned.1.call-update
  8.7 0.7 all-gather.10.cloned.1.call-update
  9.4 0.5 all-gather.12.cloned.1.call-update
  10.0 0.5 all-gather.14.cloned.1.call-update
  10.8 33.3 %all_gather.24 = bf16[2048,128]{1,0:T(8,128)(2,1)S(1)} all-gather(bf16[256,128]{1,0:T(8,128)(2,1)} %param.13), channel_id=1, replica_groups=mesh['sp'=8,'tp'=4] {'sp'}, dimensions={0}, use_global_device_ids=true | all-gather | bytes 589824 | tf_op jit(solution)/shard_map/all_gather | solution.py:134
  44.1 32.2 %all_gather.25 = bf16[2048,128]{1,0:T(8,128)(2,1)S(1)} all-gather(bf16[256,128]{1,0:T(8,128)(2,1)} %param.14), channel_id=1, replica_groups=mesh['sp'=8,'tp'=4] {'sp'}, dimensions={0}, use_global_device_ids=true | all-gather | bytes 589824 | tf_op jit(solution)/shard_map/all_gather | solution.py:135
  76.3 0.7 max.38
  77.0 0.9 multiply_cosine_fusion.1
  78.5 0.7 convert_add_fusion
  79.2 2.2 fusion
  81.5 2.5 convolution_convert_fusion.4
  84.1 2.0 convolution_convert_fusion.2
  86.1 4.0 %collective-permute-start = (bf16[8,256]{1,0:T(8,128)(2,1)S(1)}, bf16[8,256]{1,0:T(8,128)(2,1)}, u32[]{:S(2)}, u32[]{:S(2)}) collective-permute-start(bf16[8,256]{1,0:T(8,128)(2,1)S(1)} %get-tuple-element.41), channel_id=1, source_target_pairs={{0,4},{4,8},{8,12},{12,16},{16,20},{20,24},{24,28},{1,5},{5,9},{9,... | collective-permute-start | bytes 12296 | tf_op jit(solution)/shard_map/ppermute | solution.py:25
  90.1 1.3 collective-permute-start.1
  91.5 1.6 convolution_convert_fusion.3
  93.1 4.6 %collective-permute-start.2 = (bf16[128,256]{0,1:T(8,128)(2,1)S(1)}, bf16[128,256]{0,1:T(8,128)(2,1)S(1)}, u32[]{:S(2)}, u32[]{:S(2)}) collective-permute-start(bf16[128,256]{0,1:T(8,128)(2,1)S(1)} %get-tuple-element.37), channel_id=1, source_target_pairs={{0,4},{4,8},{8,12},{12,16},{16,20},{20,24},{24,28},{1,5},{5,9},{9,... | collective-permute-start | bytes 196616 | tf_op jit(solution)/shard_map/ppermute | solution.py:25
  97.7 1.5 collective-permute-start.3
  99.1 21.1 %all-gather.10.cloned.1.call-done = bf16[256,2048]{1,0:T(8,128)(2,1)} async-done(((bf16[256,256]{1,0:T(8,128)(2,1)}), bf16[256,2048]{1,0:T(8,128)(2,1)}) %all-gather.10.cloned.1.call-update) | async-done | bytes 1048592 | tf_op jit(solution)/shard_map/all_gather | solution.py:106
  120.2 8.6 %fusion.11 = f32[512,2048]{1,0:T(8,128)} fusion(bf16[256,2048]{1,0:T(8,128)(2,1)} %all-gather.10.cloned.1.call-done, bf16[512,256]{1,0:T(8,128)(2,1)} %copy-done.9, bf16[8,256]{1,0:T(8,128)(2,1)} %collective-permute-done.1, bf16[8,256]{1,0:T(8,128)(2,1)} %collective-permute-done, f32[512]{0:T(512)S(1)} %get-tuple-element.2, ...), kind=kOutput, calls=%fused_computation.23 | convolution fusion | flops 616562688 | bytes 5654528 | tf_op jit(solution)/shard_map/dot_general | solution.py:182
  129.0 41.4 %all-gather.12.cloned.1.call-done = bf16[2048,512]{1,0:T(8,128)(2,1)} async-done(((bf16[256,512]{1,0:T(8,128)(2,1)}), bf16[2048,512]{1,0:T(8,128)(2,1)}) %all-gather.12.cloned.1.call-update) | async-done | bytes 2097168 | tf_op jit(solution)/shard_map/all_gather | solution.py:133
  170.3 3.0 %convolution_convert_fusion = bf16[512,512]{0,1:T(8,128)(2,1)S(1)} fusion(bf16[2048,512]{1,0:T(8,128)(2,1)} %all-gather.12.cloned.1.call-done, bf16[512,2048]{1,0:T(8,128)(2,1)S(1)} %copy-done.1, f32[2048]{0:T(1024)} %param.11, f32[512]{0:T(512)S(1)} %copy-done.7), kind=kOutput, calls=%fused_computation.18 | convolution fusion | flops 1078198272 | bytes 4728832 | tf_op jit(solution)/shard_map/dot_general | solution.py:138
  173.7 0.8 fusion.5
  174.6 0.8 fusion.6
  175.4 0.9 fusion.3
  176.4 0.9 fusion.4
  177.4 1.2 fusion.10
  178.6 1.2 fusion.9
  179.8 41.2 %all-gather.14.cloned.1.call-done = bf16[512,2048]{1,0:T(8,128)(2,1)} async-done(((bf16[512,256]{1,0:T(8,128)(2,1)}), bf16[512,2048]{1,0:T(8,128)(2,1)}) %all-gather.14.cloned.1.call-update) | async-done | bytes 2097168 | tf_op jit(solution)/shard_map/all_gather | solution.py:107
  221.1 5.5 %add_convert_fusion = bf16[512,2048]{1,0:T(8,128)(2,1)} fusion(f32[512,2048]{1,0:T(8,128)} %fusion.11, bf16[512,2048]{1,0:T(8,128)(2,1)} %all-gather.14.cloned.1.call-done, bf16[256,512]{0,1:T(8,128)(2,1)S(1)} %bitcast.79, bf16[256,512]{0,1:T(8,128)(2,1)S(1)} %bitcast.78), kind=kOutput, calls=%fused_computation.7 | convolution fusion | flops 1076887552 | bytes 8912896 | tf_op jit(solution)/shard_map/dot_general | solution.py:183
  226.8 0.6 pad_maximum_fusion.16
  227.4 28.7 %reduce-scatter.2.cloned.1.call-done = bf16[512,512]{1,0:T(8,128)(2,1)} async-done(((bf16[512,2048]{1,0:T(8,128)(2,1)}), bf16[512,512]{1,0:T(8,128)(2,1)}) %reduce-scatter.2.cloned.1.call-update) | async-done | bytes 524304 | tf_op jit(solution)/shard_map/reduce_scatter | solution.py:184
  (64 shorter events, 1.8 us)
Async XLA Ops:
  7.2 113.1 %copy-start = (bf16[1,256,256]{2,1,0:T(8,128)(2,1)S(1)}, bf16[1,256,256]{2,1,0:T(8,128)(2,1)}, u32[]{:S(2)}) copy-start(bf16[1,256,256]{2,1,0:T(8,128)(2,1)} %param.16) | copy-start | bytes 393220
  7.2 72.0 %all-gather.6.cloned.1.call-start = ((), (), s32[]{:S(2)}) async-start(), calls=%async_computation.1 | async-start | bytes 2621440 | tf_op jit(solution)/shard_map/all_gather | solution.py:123
  7.9 76.1 %all-gather.8.cloned.1.call-start = ((), (), s32[]{:S(2)}) async-start(), calls=%async_computation.2 | async-start | bytes 1179648 | tf_op jit(solution)/shard_map/all_gather | solution.py:136
  8.7 111.5 %all-gather.10.cloned.1.call-start = ((), (), s32[]{:S(2)}) async-start(), calls=%async_computation.3 | async-start | bytes 1179648 | tf_op jit(solution)/shard_map/all_gather | solution.py:106
  9.4 160.9 %all-gather.12.cloned.1.call-start = ((), (), s32[]{:S(2)}) async-start(), calls=%async_computation.4 | async-start | bytes 2359296 | tf_op jit(solution)/shard_map/all_gather | solution.py:133
  10.0 211.1 %all-gather.14.cloned.1.call-start = ((), (), s32[]{:S(2)}) async-start(), calls=%async_computation.5 | async-start | bytes 2359296 | tf_op jit(solution)/shard_map/all_gather | solution.py:107
  10.6 245.5 %reduce-scatter.2.cloned.1.call-start = ((), (), s32[]{:S(2)}) async-start(), calls=%async_computation.6 | async-start | bytes 2621440 | tf_op jit(solution)/shard_map/reduce_scatter | solution.py:184
  79.2 4.9 %copy-start.1 = (bf16[512,2048]{1,0:T(8,128)(2,1)S(1)}, bf16[512,2048]{1,0:T(8,128)(2,1)}, u32[]{:S(2)}) copy-start(bf16[512,2048]{1,0:T(8,128)(2,1)} %all-gather.6.cloned.1.call-done) | copy-start | bytes 6291460
  81.4 2.6 copy-start.6
  84.0 7.4 %copy-start.2 = (f32[512,16]{0,1:T(8,128)S(1)}, f32[512,16]{0,1:T(8,128)}, u32[]{:S(2)}) copy-start(f32[512,16]{0,1:T(8,128)} %get-tuple-element.43) | copy-start | bytes 98308
  84.0 7.4 %copy-start.3 = (f32[512,16]{0,1:T(8,128)S(1)}, f32[512,16]{0,1:T(8,128)}, u32[]{:S(2)}) copy-start(f32[512,16]{0,1:T(8,128)} %get-tuple-element.44) | copy-start | bytes 98308
  84.0 7.4 %copy-start.4 = (f32[512,16]{0,1:T(8,128)S(1)}, f32[512,16]{0,1:T(8,128)}, u32[]{:S(2)}) copy-start(f32[512,16]{0,1:T(8,128)} %get-tuple-element.51) | copy-start | bytes 98308
  84.0 7.4 %copy-start.5 = (f32[512,16]{0,1:T(8,128)S(1)}, f32[512,16]{0,1:T(8,128)}, u32[]{:S(2)}) copy-start(f32[512,16]{0,1:T(8,128)} %get-tuple-element.52) | copy-start | bytes 98308
  84.0 7.5 %copy-start.10 = (f32[2048]{0:T(1024)S(1)}, f32[2048]{0:T(1024)}, u32[]{:S(2)}) copy-start(f32[2048]{0:T(1024)} %param.11) | copy-start | bytes 24580
  86.1 5.4 %copy-start.9 = (bf16[512,256]{1,0:T(8,128)(2,1)}, bf16[512,256]{1,0:T(8,128)(2,1)S(1)}, u32[]{:S(2)}) copy-start(bf16[512,256]{1,0:T(8,128)(2,1)S(1)} %convolution_convert_fusion.2) | copy-start | bytes 786436
  86.1 34.1 %collective-permute-start = (bf16[8,256]{1,0:T(8,128)(2,1)S(1)}, bf16[8,256]{1,0:T(8,128)(2,1)}, u32[]{:S(2)}, u32[]{:S(2)}) collective-permute-start(bf16[8,256]{1,0:T(8,128)(2,1)S(1)} %get-tuple-element.41), channel_id=1, source_target_pairs={{0,4},{4,8},{8,12},{12,16},{16,20},{20,24},{24,28},{1,5},{5,9},{9,... | collective-permute-start | bytes 12296 | tf_op jit(solution)/shard_map/ppermute | solution.py:25
  90.1 30.1 %collective-permute-start.1 = (bf16[8,256]{1,0:T(8,128)(2,1)S(1)}, bf16[8,256]{1,0:T(8,128)(2,1)}, u32[]{:S(2)}, u32[]{:S(2)}) collective-permute-start(bf16[8,256]{1,0:T(8,128)(2,1)S(1)} %get-tuple-element.42), channel_id=1, source_target_pairs={{4,0},{8,4},{12,8},{16,12},{20,16},{24,20},{28,24},{5,1},{9,5},{13... | collective-permute-start | bytes 12296 | tf_op jit(solution)/shard_map/ppermute | solution.py:27
  93.1 35.8 %collective-permute-start.2 = (bf16[128,256]{0,1:T(8,128)(2,1)S(1)}, bf16[128,256]{0,1:T(8,128)(2,1)S(1)}, u32[]{:S(2)}, u32[]{:S(2)}) collective-permute-start(bf16[128,256]{0,1:T(8,128)(2,1)S(1)} %get-tuple-element.37), channel_id=1, source_target_pairs={{0,4},{4,8},{8,12},{12,16},{16,20},{20,24},{24,28},{1,5},{5,9},{9,... | collective-permute-start | bytes 196616 | tf_op jit(solution)/shard_map/ppermute | solution.py:25
  97.7 31.2 %collective-permute-start.3 = (bf16[128,256]{0,1:T(8,128)(2,1)S(1)}, bf16[128,256]{0,1:T(8,128)(2,1)S(1)}, u32[]{:S(2)}, u32[]{:S(2)}) collective-permute-start(bf16[128,256]{0,1:T(8,128)(2,1)S(1)} %get-tuple-element.38), channel_id=1, source_target_pairs={{4,0},{8,4},{12,8},{16,12},{20,16},{24,20},{28,24},{5,1},{9,5},{13... | collective-permute-start | bytes 196616 | tf_op jit(solution)/shard_map/ppermute | solution.py:27
  120.2 50.1 %copy-start.7 = (f32[512]{0:T(512)S(1)}, f32[512]{0:T(512)}, u32[]{:S(2)}) copy-start(f32[512]{0:T(512)} %copy-done.6) | copy-start | bytes 6148
  221.1 5.6 %copy-start.8 = (f32[8]{0:T(128)S(1)}, f32[8]{0:T(128)}, u32[]{:S(2)}) copy-start(f32[8]{0:T(128)} %param.17) | copy-start | bytes 100
Sparse Core Ops, SparseCore 0:
  9.5 25.2 all-gather.5
  37.0 41.2 all-gather.7
  80.3 39.8 all-gather.9
  122.2 48.0 all-gather.11
  172.2 48.8 all-gather.13
  226.7 29.3 reduce-scatter.1
where the time goes:
time: 263 us
  waiting for transfers between devices  136 us (52%)
  blocking collectives  65.5 us (25%)
  matrix products  27.4 us (10%)
  between operations  14.6 us (6%)
  starting transfers between devices  11.5 us (4%)
  other arithmetic  7.62 us (3%)
    all_gather x1, waiting for transfers between devices, local(): lax.all_gather(weights_in[0], 'sp', axis=0, tiled=True)  41.4 us
    all_gather x1, waiting for transfers between devices, fetch_outputs(): lax.all_gather(out_attn_weight, 'sp', axis=1, tiled=True)  41.2 us
    all_gather x1, blocking collectives, local(): lax.all_gather(weights_in[1], 'sp', axis=0, tiled=True)  33.3 us
    all_gather x1, blocking collectives, local(): lax.all_gather(weights_in[2], 'sp', axis=0, tiled=True)  32.2 us
    reduce_scatter x1, waiting for transfers between devices, local(): lax.psum_scatter(term.astype(jnp.bfloat16), 'tp', scatter_dimension=1, ti...  28.7 us
    all_gather x1, waiting for transfers between devices, fetch_outputs(): lax.all_gather(out_pool_weight, 'sp', axis=1, tiled=True)  21.1 us
    dot_general x4, matrix products, local(): jnp.dot(normed, piece, preferred_element_type=jnp.float32)  9.08 us
    dot_general x1, matrix products, local(): term = jnp.dot(pool_out, out_pool_full, preferred_element_type=jnp.float32)  8.65 us
  transfers between devices with their start and end apart: 10, of which 4 were waited for; matrix products, arithmetic and copies ran while one was open for 12% of the time, Pallas kernels for 0%

commit v1 on v0

--- a/solution.py
+++ b/solution.py
@@ -1,6 +1,10 @@
+import functools
+
 import jax
 import jax.numpy as jnp
 from jax import lax
+from jax.experimental import pallas as pl
+from jax.experimental.pallas import tpu as pltpu
 from jax.sharding import PartitionSpec as P
 
 HD = 64
@@ -99,6 +103,38 @@
     weights = (exps / row_total[..., None]).astype(jnp.bfloat16)
     attended = jnp.einsum("hgqk,khd->qhgd", weights, values, preferred_element_type=jnp.float32)
     return (attended.astype(jnp.bfloat16), row_top + jnp.log(row_total))
+
+
+def attend_all(rot_query, key_ext, value_ext, sink_logit, offset, seq_total):
+    tok_rows = rot_query.shape[0]
+    heads_local = rot_query.shape[1] // HD
+    kv_local = key_ext.shape[1] // HD
+    grp = heads_local // kv_local
+    query_heads = rot_query.reshape(tok_rows, kv_local, grp, HD)
+    key_heads = key_ext.reshape(-1, kv_local, HD)
+    value_heads = value_ext.reshape(-1, kv_local, HD)
+    sink = sink_logit.reshape(kv_local, grp)
+    block_rows = min(tok_rows, 256)
+    attended_parts = []
+    log_parts = []
+    for block_index in range(tok_rows // block_rows):
+        start = block_index * block_rows
+        query_pos = offset + start + jnp.arange(block_rows, dtype=jnp.int32)
+        key_pos = offset + start - WINDOW + jnp.arange(block_rows + 2 * WINDOW, dtype=jnp.int32)
+        attended_block, log_block = attend_block(
+            query_heads[start : start + block_rows],
+            key_heads[start : start + block_rows + 2 * WINDOW],
+            value_heads[start : start + block_rows + 2 * WINDOW],
+            sink,
+            query_pos,
+            key_pos,
+            seq_total,
+        )
+        attended_parts.append(attended_block.reshape(block_rows, heads_local * HD))
+        log_parts.append(log_block.reshape(heads_local, block_rows))
+    attended = jnp.concatenate(attended_parts, 0)
+    log_weight = jnp.concatenate(log_parts, 1)
+    return (attended, log_weight)
 
 
 def fetch_outputs(out_pool_weight, out_attn_weight):
@@ -151,33 +187,7 @@
     pool_out = jnp.dot(pooled, pool_mix_weight[0], preferred_element_type=jnp.float32).astype(
         jnp.bfloat16
     )
-    heads_local = rot_query.shape[1] // HD
-    kv_local = key_width // HD
-    grp = heads_local // kv_local
-    query_heads = rot_query.reshape(tok_rows, kv_local, grp, HD)
-    key_heads = key_ext.reshape(-1, kv_local, HD)
-    value_heads = value_ext.reshape(-1, kv_local, HD)
-    sink = sink_logit.reshape(kv_local, grp)
-    block_rows = min(tok_rows, 256)
-    attended_parts = []
-    log_parts = []
-    for block_index in range(tok_rows // block_rows):
-        start = block_index * block_rows
-        query_pos = offset + start + jnp.arange(block_rows, dtype=jnp.int32)
-        key_pos = offset + start - WINDOW + jnp.arange(block_rows + 2 * WINDOW, dtype=jnp.int32)
-        attended_block, log_block = attend_block(
-            query_heads[start : start + block_rows],
-            key_heads[start : start + block_rows + 2 * WINDOW],
-            value_heads[start : start + block_rows + 2 * WINDOW],
-            sink,
-            query_pos,
-            key_pos,
-            seq_total,
-        )
-        attended_parts.append(attended_block.reshape(block_rows, heads_local * HD))
-        log_parts.append(log_block.reshape(heads_local, block_rows))
-    attended = jnp.concatenate(attended_parts, 0)
-    log_weight = jnp.concatenate(log_parts, 1)
+    attended, log_weight = attend_all(rot_query, key_ext, value_ext, sink_logit, offset, seq_total)
     out_pool_full, out_attn_full = fetch_outputs(out_pool_weight, out_attn_weight)
     term = jnp.dot(pool_out, out_pool_full, preferred_element_type=jnp.float32)
     term = term + jnp.dot(attended, out_attn_full, preferred_element_type=jnp.float32)
@@ -185,9 +195,329 @@
     return (mixed, log_weight)
 
 
+def make_perm(planes, rule):
+    pairs = []
+    for z in range(planes):
+        for y in range(2):
+            for x in range(2):
+                for c in range(2):
+                    to = rule(z, y, x, c)
+                    if to is not None:
+                        pairs.append((lin(z, y, x, c), lin(*to)))
+    return pairs
+
+
+def lin(z, y, x, c):
+    return ((z * 2 + y) * 2 + x) * 2 + c
+
+
+def send(value, rule, planes=4):
+    return lax.ppermute(value, ("sp", "tp"), make_perm(planes, rule))
+
+
+def after(value, *tokens):
+    return lax.optimization_barrier((value, *tokens))[0]
+
+
+def swap_away(z, y, x, c):
+    return (z, c, x, y) if y != c else None
+
+
+def home_to_away(z, y, x, c):
+    return (z, y, x, 1 - c) if y == c else None
+
+
+def away_to_home(z, y, x, c):
+    return (z, y, x, 1 - c) if y != c else None
+
+
+def other_core(z, y, x, c):
+    return (z, y, x, 1 - c)
+
+
+def line_one(z, y, x, c):
+    if c == 0:
+        return (z + 1, y, x, c) if z < 3 else None
+    return (z - 1, y, x, c) if z > 0 else None
+
+
+def line_two(core):
+    def rule(z, y, x, c):
+        if z not in (1, 2):
+            return None
+        return (z + 1 if c == 0 else z - 1, y, x, core)
+
+    return rule
+
+
+def line_three(core):
+    def rule(z, y, x, c):
+        if c != core or z not in (1, 2):
+            return None
+        return (0 if z == 1 else 3, y, x, c)
+
+    return rule
+
+
+def token_one(z, y, x, c):
+    return (z, y, 1 - x, c) if y == c else (z, 1 - y, x, 1 - c)
+
+
+def token_two(z, y, x, c):
+    return (z, y, 1 - x, 1 - c) if y != c else (z, 1 - y, x, c)
+
+
+def token_diag(z, y, x, c):
+    return (z, y, 1 - x, c) if y != c else None
+
+
+def halo_next(z, y, x, c):
+    if c == 0:
+        return (z, y, x, 1)
+    return (z + 1, y, x, 0) if z < 3 else None
+
+
+def halo_prev(z, y, x, c):
+    if c == 1:
+        return (z, y, x, 0)
+    return (z - 1, y, x, 1) if z > 0 else None
+
+
+def norm_kernel(idx, own, p1, p2, p3, p4, p5, gain, out, buf, sems):
+    home = idx[0]
+    places = [idx[1], idx[2], idx[3], idx[4]]
+    at_home = (own, p3, p1, p2)
+    at_away = (p2, p1, p5, p4)
+    for which in range(4):
+
+        @pl.when(home == 1)
+        def _():
+            pltpu.make_async_copy(at_home[which], buf.at[places[which]], sems.at[which]).start()
+
+        @pl.when(home == 0)
+        def _():
+            pltpu.make_async_copy(at_away[which], buf.at[places[which]], sems.at[which]).start()
+
+    for which in range(4):
+        pltpu.make_async_copy(own, buf.at[places[which]], sems.at[which]).wait()
+    blocks, rows, wide = buf.shape
+    half = wide // 2
+    step = 128
+
+    def body(i, carry):
+        at = pl.ds(pl.multiple_of(i * step, step), step)
+        total = jnp.zeros((step, 1), jnp.float32)
+        for b in range(blocks):
+            v = buf[b, at, :].astype(jnp.float32)
+            total = total + jnp.sum(v * v, -1, keepdims=True)
+        scale = lax.rsqrt(total / (blocks * wide) + norm_eps)
+        for b in range(blocks):
+            v = buf[b, at, :].astype(jnp.float32)
+            buf[b, at, :] = (v * scale * gain[:, b * wide : (b + 1) * wide]).astype(jnp.bfloat16)
+        for slot in range(out.shape[0]):
+            fb = idx[5 + slot]
+            col = pl.multiple_of((fb % 2) * half, half)
+            out[slot, at, :] = buf[fb // 2, at, pl.ds(col, half)]
+        return carry
+
+    lax.fori_loop(0, rows // step, body, 0)
+
+
+def normed_slots(idx, pieces, gain, slots):
+    rows, wide = pieces[0].shape
+    anyspace = pl.BlockSpec(memory_space=pl.ANY)
+    return pl.pallas_call(
+        norm_kernel,
+        out_shape=jax.ShapeDtypeStruct((slots, rows, wide // 2), jnp.bfloat16),
+        in_specs=[pl.BlockSpec(memory_space=pltpu.SMEM)] + [anyspace] * 6 + [pl.BlockSpec(memory_space=pltpu.VMEM)],
+        out_specs=pl.BlockSpec(memory_space=pltpu.VMEM),
+        scratch_shapes=[pltpu.VMEM((4, rows, wide), jnp.bfloat16), pltpu.SemaphoreType.DMA((4,))],
+        name="norm",
+    )(idx, *pieces, gain)
+
+
+def gather_dot(first, has_acc, *refs):
+    normed = refs[0]
+    count = len(refs) - 2 - (1 if has_acc else 0)
+    weights = refs[1 : 1 + count]
+    out = refs[-1]
+    rows = normed.shape[1]
+    step = 256
+    for at in range(0, rows, step):
+        total = refs[1 + count][at : at + step] if has_acc else None
+        for i in range(count):
+            part = jnp.dot(normed[first + i, at : at + step, :], weights[i][...], preferred_element_type=jnp.float32)
+            total = part if total is None else total + part
+        out[at : at + step] = total
+
+
+def project(normed, first, weights, acc):
+    rows = normed.shape[1]
+    cols = weights[0].shape[1]
+    args = (normed, *weights) + (() if acc is None else (acc,))
+    return pl.pallas_call(
+        functools.partial(gather_dot, first, acc is not None),
+        out_shape=jax.ShapeDtypeStruct((rows, cols), jnp.float32),
+        name="project",
+    )(*args)
+
+
+def out_kernel(first, count, idx, acts, *refs):
+    weights = refs[:count]
+    outs = refs[-4:]
+    for i in range(count):
+        place = idx[first + i]
+        result = jnp.dot(acts[...], weights[i][...], preferred_element_type=jnp.float32).astype(jnp.bfloat16)
+        half = result.shape[1]
+        col = pl.multiple_of((place % 2) * half, half)
+        for r in range(4):
+
+            @pl.when(place // 2 == r)
+            def _():
+                outs[r][:, pl.ds(col, half)] = result
+
+
+def out_blocks(idx, acts, weights):
+    rows = acts.shape[0]
+    wide = weights[0].shape[1] * 2
+    count = len(weights)
+    return pl.pallas_call(
+        functools.partial(out_kernel, 0, count),
+        out_shape=[jax.ShapeDtypeStruct((rows, wide), jnp.bfloat16)] * 4,
+        in_specs=[pl.BlockSpec(memory_space=pltpu.SMEM)] + [pl.BlockSpec(memory_space=pltpu.VMEM)] * (1 + count),
+        out_specs=[pl.BlockSpec(memory_space=pltpu.VMEM)] * 4,
+        name="outproj",
+    )(idx, acts, *weights)
+
+
+def line_gather(own, swapped, home, core):
+    near = jnp.where(home, own, send(own, home_to_away))
+    d1 = send(near, line_one)
+    far = jnp.where(home, send(swapped, away_to_home), swapped)
+    s1 = send(far, line_one)
+    d2 = send(d1, line_two(0))
+    s2 = send(s1, line_two(1))
+    d3 = send(d2, line_three(0))
+    s3 = send(s2, line_three(1))
+    w2 = jnp.where(core == 0, d2, s2)
+    w3 = jnp.where(core == 0, d3, s3)
+    return (near, far, d1, s1, send(d1, other_core), send(s1, other_core), w2, send(w2, other_core), w3, send(w3, other_core))
+
+
+def local_lines(
+    tokens,
+    norm_gain,
+    query_weight,
+    key_weight,
+    value_weight,
+    pool_in_weight,
+    pool_mix_weight,
+    sink_logit,
+    out_pool_weight,
+    out_attn_weight,
+):
+    s, t = lax.axis_index("sp"), lax.axis_index("tp")
+    z, y, x, c = s // 2, s % 2, t // 2, t % 2
+    home = y == c
+    planes = lax.axis_size("sp") // 2
+    tok_rows = tokens.shape[0]
+    seq_total = tok_rows * lax.axis_size("sp")
+    offset = (2 * z + c) * tok_rows
+
+    w_in = jnp.concatenate([query_weight, key_weight, value_weight, pool_in_weight], 1)
+    in_swapped = send(w_in, swap_away)
+    w_slots = line_gather(w_in, in_swapped, home, c)
+
+    p1 = send(tokens, token_one)
+    p2 = send(tokens, token_two)
+    p3 = send(tokens, away_to_home)
+    p4 = send(p1, token_diag)
+    p5 = send(p2, token_diag)
+
+    w_out = jnp.concatenate([out_pool_weight, out_attn_weight, pool_mix_weight[0]], 0)
+    out_swapped = send(w_out, swap_away)
+    sink_other = send(sink_logit, swap_away)
+    mix_rows = pool_mix_weight.shape[1]
+    cut = w_out.shape[0] - mix_rows
+    mix = jnp.where(home, w_out[cut:], out_swapped[cut:])
+    sink_own = jnp.where(home, sink_logit, sink_other)
+    o_slots = line_gather(w_out[:cut], out_swapped[:cut], home, c)
+
+    zr = jnp.where(c == 0, z - 1, z + 1)
+    ze = jnp.where(c == 0, z + 1, z - 1)
+    z2 = jnp.where(z < planes // 2, z + 2, z - 2)
+    z3 = planes - 1 - z
+    yc = (y + c) % 2
+    feature = jnp.stack(
+        [
+            2 * z + y,
+            2 * z + 1 - y,
+            2 * zr + y,
+            2 * zr + 1 - y,
+            2 * ze + y,
+            2 * ze + 1 - y,
+            2 * z2 + yc,
+            2 * z2 + 1 - yc,
+            2 * z3 + yc,
+            2 * z3 + 1 - yc,
+        ]
+    )
+    outer = (z == 0) | (z == planes - 1)
+    zs = jnp.stack([z, z, zr, zr, ze, ze, z2, z2, jnp.where(outer, z3, -1), jnp.where(outer, z3, -1)])
+    valid = (zs >= 0) & (zs < planes)
+    fb = jnp.where(valid, feature, 0).astype(jnp.int32)
+    head = jnp.stack([home.astype(jnp.int32), 2 * x + c, 2 * x + 1 - c, 2 * (1 - x) + c, 2 * (1 - x) + 1 - c]).astype(jnp.int32)
+    normed = normed_slots(jnp.concatenate([head, fb]), (tokens, p1, p2, p3, p4, p5), norm_gain[None, :], 10)
+
+    acc = project(normed, 0, w_slots[:6], None)
+    sums = project(normed, 6, w_slots[6:], acc).astype(jnp.bfloat16)
+    q_w, kv_w = query_weight.shape[1], key_weight.shape[1]
+    query = sums[:, :q_w]
+    key = sums[:, q_w : q_w + kv_w]
+    value = sums[:, q_w + kv_w : q_w + 2 * kv_w]
+    pool_input = sums[:, q_w + 2 * kv_w :]
+
+    positions = offset + jnp.arange(tok_rows, dtype=jnp.int32)
+    tables = rope_tables(positions, HD)
+    rot_query = rotate_heads(query, tables, HD)
+    rot_key = rotate_heads(key, tables, HD)
+    pair = jnp.concatenate([rot_key, value], 1)
+    low = jnp.concatenate([pair[:WINDOW], pool_input[:pool_reach]], 0)
+    high = jnp.concatenate([pair[tok_rows - WINDOW :], pool_input[tok_rows - pool_reach :]], 0)
+    before = send(high, halo_next)
+    behind = send(low, halo_prev)
+    pair_ext = jnp.concatenate([before[:WINDOW], pair, behind[:WINDOW]], 0)
+    pool_ext = jnp.concatenate([before[WINDOW:], pool_input, behind[WINDOW:]], 0)
+    half_width = jnp.left_shift(jnp.int32(1), 2 * x + y)
+    pooled = pool_group(pool_ext, pool_input, positions, half_width, seq_total)
+    pool_out = jnp.dot(pooled, mix, preferred_element_type=jnp.float32).astype(jnp.bfloat16)
+    attended, log_here = attend_all(rot_query, pair_ext[:, :kv_w], pair_ext[:, kv_w:], sink_own, offset, seq_total)
+    log_weight = jnp.where(home, log_here, send(log_here, swap_away))
+
+    acts = jnp.concatenate([pool_out, attended], 1)
+    round_of = lambda zz: zz ^ (2 * x + y)
+    parity = fb % 2
+    place = jnp.where(valid, (zs ^ (2 * x + y)) * 2 + parity, -2).astype(jnp.int32)
+    blocks = out_blocks(place, acts, o_slots)
+
+    def direct(r):
+        def rule(z, y, x, c):
+            j = (2 * x + y) ^ r
+            to = (z, c, j // 2, j % 2)
+            return None if to == (z, y, x, c) else to
+
+        return rule
+
+    parts = [send(blocks[r], direct(r)) for r in range(4)]
+    parts[0] = jnp.where(home, blocks[0], parts[0])
+    mixed = sum(part.astype(jnp.float32) for part in parts).astype(jnp.bfloat16)
+    return (mixed, log_weight)
+
+
 def solution(mesh):
+    lines = mesh.shape["sp"] == 8 and mesh.shape["tp"] == 4
     return jax.shard_map(
-        local,
+        local_lines if lines else local,
         mesh=mesh,
         in_specs=(
             P("sp", "tp"),

time: 263 us -> 188 us (0.71); the launches traced: 263 us -> 185 us
  waiting for transfers between devices: 136 us -> 26.8 us
  blocking collectives: 65.5 us -> 0 us
  starting transfers between devices: 11.5 us -> 76.1 us
  Pallas kernels: 0 us -> 25.7 us
  other arithmetic: 7.62 us -> 25.7 us
  local copies, waits for them, and re-layouts: 0.88 us -> 15.4 us
  matrix products: 27.4 us -> 13.7 us
  between operations: 14.6 us -> 1.74 us
    all_gather x5 -> x0, waiting for transfers between devices: 104 us -> none  [the longest x1 41.4 us: local(): lax.all_gather(weights_in[0], 'sp', axis=0, tiled=True)]
    all_gather x2 -> x0, blocking collectives: 65.5 us -> none  [the longest x1 33.3 us: local(): lax.all_gather(weights_in[1], 'sp', axis=0, tiled=True)]
    ppermute x4 -> x39, starting transfers between devices: 11.3 us -> 76.1 us  [send(): return lax.ppermute(value, ('sp', 'tp'), make_perm(planes, rule))]
    reduce_scatter x1 -> x0, waiting for transfers between devices: 28.7 us -> none  [local(): lax.psum_scatter(term.astype(jnp.bfloat16), 'tp', scatter_dimension=1, ti...]
    ppermute x4 -> x39, waiting for transfers between devices: 0.01 us -> 26.8 us  [send(): return lax.ppermute(value, ('sp', 'tp'), make_perm(planes, rule))]
    pallas_call x0 -> x4, Pallas kernels: none -> 25.7 us  [the longest x2 11.4 us: project(): pl.pallas_call(functools.partial(gather_dot, first, acc is not None), out...]
    dot_general x6 -> x1, matrix products: 23.2 us -> 3.25 us  [local_lines(): jnp.dot(pooled, mix, preferred_element_type=jnp.float32)]
    select_n x0 -> x11, other arithmetic: none -> 9.12 us  [the longest x2 2.92 us: line_gather(): w2 = jnp.where(core == 0, d2, s2)]
  transfers between devices with their start and end apart: 10 -> 39, of which waited for: 4 -> 5; matrix products, arithmetic and copies ran while one was open for 12% -> 24% of each run, Pallas kernels for 0% -> 9%
where the time goes in v1:
time: 188 us; the launch traced here: 185 us
  starting transfers between devices  76.1 us (40%)
  waiting for transfers between devices  26.8 us (14%)
  other arithmetic  25.7 us (14%)
  Pallas kernels  25.7 us (14%)
  local copies, waits for them, and re-layouts  15.4 us (8%)
  matrix products  13.7 us (7%)
    ppermute x39, starting transfers between devices, send(): return lax.ppermute(value, ('sp', 'tp'), make_perm(planes, rule))  76.1 us
    ppermute x39, waiting for transfers between devices, send(): return lax.ppermute(value, ('sp', 'tp'), make_perm(planes, rule))  26.8 us
    pallas_call x2, Pallas kernels, project(): pl.pallas_call(functools.partial(gather_dot, first, acc is not None), out...  11.4 us
    pallas_call x1, Pallas kernels, out_blocks(): pl.pallas_call(functools.partial(out_kernel, 0, count), out_shape=[jax.Sh...  9.39 us
    unnamed x96, local copies, waits for them, and re-layouts  7.36 us
    dot_general x2, matrix products, attend_block(): jnp.einsum('hgqk,khd->qhgd', weights, values, preferred_element_type=jnp....  6.84 us
    pallas_call x1, Pallas kernels, normed_slots(): pl.pallas_call(norm_kernel, out_shape=jax.ShapeDtypeStruct((slots, rows,...  4.94 us
    reduce_sum x2, other arithmetic, attend_block(): row_total = jnp.sum(exps, -1) + jnp.exp(sink[:, :, None] - row_top)  3.94 us
  transfers between devices with their start and end apart: 39, of which 5 were waited for; matrix products, arithmetic and copies ran while one was open for 24% of the time, Pallas kernels for 9%

profile of v1, /device:TPU:0, one launch (start us, length us, event | category | flops | bytes accessed | tf_op | source)
XLA Modules:
  0.0 185.1 jit_solution(17757546757378784732)
XLA Ops:
  4.3 3.2 %collective-permute-start.5 = (bf16[256,1024]{1,0:T(8,128)(2,1)S(1)}, bf16[256,1024]{1,0:T(8,128)(2,1)}, u32[]{:S(2)}, u32[]{:S(2)}) collective-permute-start(bf16[256,1024]{1,0:T(8,128)(2,1)S(1)} %constant_dynamic-update-slice_fusion), channel_id=1, source_target_pairs={{0,1},{2,3},{5,4},{7,6},{8,9},{10,11},{13,12},{15,14},{16,17},{18,... | collective-permute-start | bytes 1572872 | tf_op jit(solution)/shard_map/ppermute | solution.py:215
  9.0 2.3 %collective-permute-start = (bf16[512,512]{1,0:T(8,128)(2,1)}, bf16[512,512]{1,0:T(8,128)(2,1)S(1)}, u32[]{:S(2)}, u32[]{:S(2)}) collective-permute-start(bf16[512,512]{1,0:T(8,128)(2,1)} %own.1), channel_id=1, source_target_pairs={{0,2},{1,4},{2,0},{3,6},{4,1},{5,7},{6,3},{7,5},{8,10},{9,12},{10,... | collective-permute-start | bytes 1572872 | tf_op jit(solution)/shard_map/ppermute | solution.py:215
  11.3 1.9 %pad_maximum_fusion = bf16[1024,256]{1,0:T(8,128)(2,1)} fusion(bf16[256,256]{1,0:T(8,128)(2,1)} %bitcast.96, bf16[512,256]{1,0:T(8,128)(2,1)} %param.19, bf16[256,256]{1,0:T(8,128)(2,1)} %param.18), kind=kLoop, calls=%fused_computation.42 | loop fusion | flops 1572864 | bytes 1048576 | tf_op jit(solution)/shard_map/concatenate | solution.py:437
  15.8 4.3 %collective-permute-start.22 = (bf16[768,256]{1,0:T(8,128)(2,1)S(1)}, bf16[768,256]{1,0:T(8,128)(2,1)S(1)}, u32[]{:S(2)}, u32[]{:S(2)}) collective-permute-start(bf16[768,256]{1,0:T(8,128)(2,1)S(1)} %constant_dynamic-update-slice_fusion.4), channel_id=1, source_target_pairs={{0,1},{2,3},{5,4},{7,6},{8,9},{10,11},{13,12},{15,14},{16,17},{18,... | collective-permute-start | bytes 1179656 | tf_op jit(solution)/shard_map/ppermute | solution.py:215
  22.5 4.3 %collective-permute-start.6 = (bf16[256,1024]{1,0:T(8,128)(2,1)S(1)}, bf16[256,1024]{1,0:T(8,128)(2,1)}, u32[]{:S(2)}, u32[]{:S(2)}) collective-permute-start(bf16[256,1024]{1,0:T(8,128)(2,1)S(1)} %broadcast_select_fusion.1.refs_1_), channel_id=1, source_target_pairs={{0,8},{2,10},{4,12},{6,14},{8,16},{9,1},{10,18},{11,3},{12,20},{13... | collective-permute-start | bytes 1572872 | tf_op jit(solution)/shard_map/ppermute | solution.py:215
  28.1 3.6 %collective-permute-start.10 = (bf16[256,1024]{1,0:T(8,128)(2,1)S(1)}, bf16[256,1024]{1,0:T(8,128)(2,1)}, u32[]{:S(2)}, u32[]{:S(2)}) collective-permute-start(bf16[256,1024]{1,0:T(8,128)(2,1)S(1)} %broadcast_select_fusion.refs_2_), channel_id=1, source_target_pairs={{0,8},{2,10},{4,12},{6,14},{8,16},{9,1},{10,18},{11,3},{12,20},{13... | collective-permute-start | bytes 1572872 | tf_op jit(solution)/shard_map/ppermute | solution.py:215
  37.2 7.1 %collective-permute-start.1 = (bf16[512,512]{1,0:T(8,128)(2,1)S(1)}, bf16[512,512]{1,0:T(8,128)(2,1)S(1)}, u32[]{:S(2)}, u32[]{:S(2)}) collective-permute-start(bf16[512,512]{1,0:T(8,128)(2,1)S(1)} %copy-done.16), channel_id=1, source_target_pairs={{0,4},{1,2},{2,6},{3,0},{4,7},{5,1},{6,5},{7,3},{8,12},{9,10},{10,... | collective-permute-start | bytes 1572872 | tf_op jit(solution)/shard_map/ppermute | solution.py:215
  52.4 7.3 %collective-permute-start.24 = (bf16[768,256]{1,0:T(8,128)(2,1)S(1)}, bf16[768,256]{1,0:T(8,128)(2,1)}, u32[]{:S(2)}, u32[]{:S(2)}) collective-permute-start(bf16[768,256]{1,0:T(8,128)(2,1)S(1)} %broadcast_select_fusion.7.refs_0_), channel_id=1, source_target_pairs={{0,8},{2,10},{4,12},{6,14},{8,16},{9,1},{10,18},{11,3},{12,20},{13... | collective-permute-start | bytes 1179656 | tf_op jit(solution)/shard_map/ppermute | solution.py:215
  59.7 2.1 %collective-permute-start.25 = (bf16[768,256]{1,0:T(8,128)(2,1)S(1)}, bf16[768,256]{1,0:T(8,128)(2,1)}, u32[]{:S(2)}, u32[]{:S(2)}) collective-permute-start(bf16[768,256]{1,0:T(8,128)(2,1)S(1)} %broadcast_select_fusion.6.refs_1_), channel_id=1, source_target_pairs={{0,8},{2,10},{4,12},{6,14},{8,16},{9,1},{10,18},{11,3},{12,20},{13... | collective-permute-start | bytes 1179656 | tf_op jit(solution)/shard_map/ppermute | solution.py:215
  66.9 1.6 collective-permute-done.25.refs_3_
  68.5 3.4 %collective-permute-start.16 = (bf16[256,1024]{1,0:T(8,128)(2,1)}, bf16[256,1024]{1,0:T(8,128)(2,1)}, u32[]{:S(2)}, u32[]{:S(2)}) collective-permute-start(bf16[256,1024]{1,0:T(8,128)(2,1)} %collective-permute-done.6.refs_3_), channel_id=1, source_target_pairs={{0,1},{1,0},{2,3},{3,2},{4,5},{5,4},{6,7},{7,6},{8,9},{9,8},{10,11... | collective-permute-start | bytes 1572872 | tf_op jit(solution)/shard_map/ppermute | solution.py:215
  74.4 2.9 %collective-permute-start.17 = (bf16[256,1024]{1,0:T(8,128)(2,1)}, bf16[256,1024]{1,0:T(8,128)(2,1)}, u32[]{:S(2)}, u32[]{:S(2)}) collective-permute-start(bf16[256,1024]{1,0:T(8,128)(2,1)} %collective-permute-done.10.refs_4_), channel_id=1, source_target_pairs={{0,1},{1,0},{2,3},{3,2},{4,5},{5,4},{6,7},{7,6},{8,9},{9,8},{10,11... | collective-permute-start | bytes 1572872 | tf_op jit(solution)/shard_map/ppermute | solution.py:215
  78.4 3.3 %collective-permute-done.28 = bf16[768,256]{1,0:T(8,128)(2,1)} collective-permute-done((bf16[768,256]{1,0:T(8,128)(2,1)}, bf16[768,256]{1,0:T(8,128)(2,1)}, u32[]{:S(2)}, u32[]{:S(2)}) %collective-permute-start.28) | collective-permute-done | bytes 393248 | tf_op jit(solution)/shard_map/ppermute | solution.py:215
  84.4 2.7 %collective-permute-start.12 = (bf16[256,1024]{1,0:T(8,128)(2,1)S(1)}, bf16[256,1024]{1,0:T(8,128)(2,1)S(1)}, u32[]{:S(2)}, u32[]{:S(2)}) collective-permute-start(bf16[256,1024]{1,0:T(8,128)(2,1)S(1)} %broadcast_select_fusion.3.refs_1_), channel_id=1, source_target_pairs={{0,1},{1,0},{2,3},{3,2},{4,5},{5,4},{6,7},{7,6},{8,9},{9,8},{10,11... | collective-permute-start | bytes 1572872 | tf_op jit(solution)/shard_map/ppermute | solution.py:215
  88.0 4.9 %norm.1.refs_0_ = bf16[10,512,256]{2,1,0:T(8,128)(2,1)} custom-call(s32[15]{0:T(128)} %concatenate.67.idx, bf16[512,512]{1,0:T(8,128)(2,1)} %own.1, bf16[512,512]{1,0:T(8,128)(2,1)} %copy-done.17, bf16[512,512]{1,0:T(8,128)(2,1)} %copy-done.18, bf16[512,512]{1,0:T(8,128)(2,1)} %copy-done.19, bf16[512,512]{1,0:T(8,128)(2,1)} %collective-permute-done.3.p4, ...), custom_call_target="tpu_custom_call" | custom-call | tf_op jit(solution)/shard_map/norm/pallas_call | solution.py:329
  92.9 1.8 broadcast_select_fusion.5.refs_6_
  95.1 5.7 %project.2.refs_5_ = f32[512,1024]{1,0:T(8,128)} custom-call(bf16[10,512,256]{2,1,0:T(8,128)(2,1)} %norm.1.refs_0_, bf16[256,1024]{1,0:T(8,128)(2,1)} %copy-done.4, bf16[256,1024]{1,0:T(8,128)(2,1)} %copy-done.5, bf16[256,1024]{1,0:T(8,128)(2,1)} %collective-permute-done.6.refs_3_, bf16[256,1024]{1,0:T(8,128)(2,1)} %collective-permute-done.10.refs_4_, ...), custom_call_target="tpu_custom_call" | custom-call | tf_op jit(solution)/shard_map/project/pallas_call | solution.py:358
  103.3 5.6 %project.3 = f32[512,1024]{1,0:T(8,128)} custom-call(bf16[10,512,256]{2,1,0:T(8,128)(2,1)} %norm.1.refs_0_, bf16[256,1024]{1,0:T(8,128)(2,1)} %copy-done.2, bf16[256,1024]{1,0:T(8,128)(2,1)} %copy-done.21, bf16[256,1024]{1,0:T(8,128)(2,1)} %copy-done.3, bf16[256,1024]{1,0:T(8,128)(2,1)} %collective-permute-done.15.refs_4_, f32[512,1024]{1,0:T(8,128)} %project.2.refs_5_), custom_call_target="tpu_custom_call" | custom-call | tf_op jit(solution)/shard_map/project/pallas_call | solution.py:358
  109.0 1.8 convert_element_type.226
  112.0 2.7 %collective-permute-start.18 = (bf16[136,256]{1,0:T(8,128)(2,1)}, bf16[136,256]{1,0:T(8,128)(2,1)}, u32[]{:S(2)}, u32[]{:S(2)}) collective-permute-start(bf16[136,256]{1,0:T(8,128)(2,1)} %get-tuple-element.49), channel_id=1, source_target_pairs={{0,1},{1,8},{2,3},{3,10},{4,5},{5,12},{6,7},{7,14},{8,9},{9,16},{1... | collective-permute-start | bytes 208904 | tf_op jit(solution)/shard_map/ppermute | solution.py:215
  117.7 3.1 %collective-permute-start.33 = (bf16[768,256]{1,0:T(8,128)(2,1)S(1)}, bf16[768,256]{1,0:T(8,128)(2,1)S(1)}, u32[]{:S(2)}, u32[]{:S(2)}) collective-permute-start(bf16[768,256]{1,0:T(8,128)(2,1)S(1)} %broadcast_select_fusion.4.refs_8_), channel_id=1, source_target_pairs={{0,1},{1,0},{2,3},{3,2},{4,5},{5,4},{6,7},{7,6},{8,9},{9,8},{10,11... | collective-permute-start | bytes 1179656 | tf_op jit(solution)/shard_map/ppermute | solution.py:215
  122.8 2.8 %fusion.2 = (f32[2,4,256]{2,1,0:T(4,128)S(1)}, f32[2,512,256,4]{2,1,3,0:T(8,128)}) fusion(pred[256,512]{0,1:T(8,128)(4,1)S(1)} %copy-done.12, bf16[512,2,64,1]{0,2,3,1:T(8,128)(2,1)S(1)} %bitcast.90, bf16[256,2,4,64]{0,3,2,1:T(8,128)(2,1)S(1)} %bitcast.87), kind=kOutput, calls=%fused_computation.8 | convolution fusion | flops 137361408 | bytes 4726784 | tf_op jit(solution)/shard_map/qhgd,khd->hgqk/dot_general | solution.py:91
  125.7 3.1 %fusion = f32[2,4,256]{2,1,0:T(4,128)S(1)} fusion(f32[2,512,256,4]{2,1,3,0:T(8,128)} %get-tuple-element.66, f32[2,4,256]{2,1,0:T(4,128)S(1)} %broadcast_maximum_fusion.1, pred[256,512]{0,1:T(8,128)(4,1)S(1)} %copy-done.12), kind=kLoop, calls=%fused_computation.6 | loop fusion | flops 4192256 | bytes 4341760 | tf_op jit(solution)/shard_map/reduce_sum | solution.py:102
  129.7 1.9 %copy-done = f32[2,512,256,4]{2,1,3,0:T(8,128)} copy-done((f32[2,512,256,4]{2,1,3,0:T(8,128)}, f32[2,512,256,4]{2,1,3,0:T(8,128)S(1)}, u32[]{:S(2)}) %copy-start) | copy-done | bytes 4194328
  132.8 3.4 %fusion.6 = bf16[2,64,4,256]{3,1,2,0:T(8,128)(2,1)S(1)} fusion(bf16[512,2,64,1]{0,2,3,1:T(8,128)(2,1)S(1)} %bitcast.95, f32[2,512,256,4]{2,1,3,0:T(8,128)} %copy-done, f32[2,4,256]{2,1,0:T(4,128)S(1)} %exponential_add_fusion, f32[2,4,256]{2,1,0:T(4,128)S(1)} %get-tuple-element.58, pred[256,512]{0,1:T(8,128)(4,1)S(1)} %copy-done.11), kind=kOutput, calls=%fused_computation.12 | convolution fusion | flops 139591680 | bytes 4734976 | tf_op jit(solution)/shard_map/hgqk,khd->qhgd/dot_general | solution.py:104
  136.6 3.4 %fusion.7 = bf16[2,64,4,256]{3,1,2,0:T(8,128)(2,1)S(1)} fusion(bf16[512,2,64,1]{0,2,3,1:T(8,128)(2,1)S(1)} %bitcast.94, f32[2,512,256,4]{2,1,3,0:T(8,128)} %get-tuple-element.66, f32[2,4,256]{2,1,0:T(4,128)S(1)} %get-tuple-element.57, f32[2,4,256]{2,1,0:T(4,128)S(1)} %broadcast_maximum_fusion.1, pred[256,512]{0,1:T(8,128)(4,1)S(1)} %copy-done.12), kind=kOutput, calls=%fused_computation.13 | convolution fusion | flops 139591680 | bytes 4734976 | tf_op jit(solution)/shard_map/hgqk,khd->qhgd/dot_general | solution.py:104
  141.7 3.2 %convolution_convert_fusion = bf16[512,256]{1,0:T(8,128)(2,1)S(1)} fusion(bf16[512,256]{1,0:T(8,128)(2,1)S(1)} %slice-done, bf16[8,256]{1,0:T(8,128)(2,1)S(1)} %slice.263, bf16[8,256]{1,0:T(8,128)(2,1)S(1)} %slice.246, f32[512]{0:T(512)S(1)} %get-tuple-element.10, pred[512]{0:T(512)(128)(4,1)S(1)} %copy-done.43, pred[512]{0:T(512)(128)(4,1)S(1)} %copy-done.42, ...), kind=kOutput, calls=%fused_computation.14 | convolution fusion | flops 79757312 | bytes 804865 | tf_op jit(solution)/shard_map/dot_general | solution.py:493
  146.7 9.4 %outproj.1 = (bf16[512,512]{1,0:T(8,128)(2,1)}, bf16[512,512]{1,0:T(8,128)(2,1)}, bf16[512,512]{1,0:T(8,128)(2,1)}, bf16[512,512]{1,0:T(8,128)(2,1)}) custom-call(s32[10]{0:T(128)} %get-tuple-element.60.idx, bf16[512,768]{1,0:T(8,128)(2,1)} %maximum_maximum_fusion.acts, bf16[768,256]{1,0:T(8,128)(2,1)} %copy-done.6, bf16[768,256]{1,0:T(8,128)(2,1)} %copy-done.7, ...), custom_call_target="tpu_custom_call" | custom-call | tf_op jit(solution)/shard_map/outproj/pallas_call | solution.py:384
  156.1 2.5 %collective-permute-start.37 = (bf16[512,512]{1,0:T(8,128)(2,1)}, bf16[512,512]{1,0:T(8,128)(2,1)S(1)}, u32[]{:S(2)}, u32[]{:S(2)}) collective-permute-start(bf16[512,512]{1,0:T(8,128)(2,1)} %get-tuple-element.9), channel_id=1, source_target_pairs={{0,3},{1,7},{2,1},{3,5},{4,2},{5,6},{6,0},{7,4},{8,11},{9,15},{10,... | collective-permute-start | bytes 1572872 | tf_op jit(solution)/shard_map/ppermute | solution.py:215
  161.8 9.9 %collective-permute-done.37 = bf16[512,512]{1,0:T(8,128)(2,1)S(1)} collective-permute-done((bf16[512,512]{1,0:T(8,128)(2,1)}, bf16[512,512]{1,0:T(8,128)(2,1)S(1)}, u32[]{:S(2)}, u32[]{:S(2)}) %collective-permute-start.37) | collective-permute-done | bytes 524320 | tf_op jit(solution)/shard_map/ppermute | solution.py:215
  171.7 11.2 %collective-permute-done.36 = bf16[512,512]{1,0:T(8,128)(2,1)S(1)} collective-permute-done((bf16[512,512]{1,0:T(8,128)(2,1)}, bf16[512,512]{1,0:T(8,128)(2,1)S(1)}, u32[]{:S(2)}, u32[]{:S(2)}) %collective-permute-start.36) | collective-permute-done | bytes 524320 | tf_op jit(solution)/shard_map/ppermute | solution.py:215
  182.9 2.2 %add_convert_fusion = bf16[512,512]{1,0:T(8,128)(2,1)} fusion(bf16[512,512]{1,0:T(8,128)(2,1)S(1)} %collective-permute-done.37, bf16[512,512]{1,0:T(8,128)(2,1)S(1)} %collective-permute-done.36, bf16[512,512]{1,0:T(8,128)(2,1)S(1)} %collective-permute-done.35, bf16[512,512]{1,0:T(8,128)(2,1)} %get-tuple-element.6, ...), kind=kLoop, calls=%fused_computation.15 | loop fusion | flops 2359296 | bytes 3145729 | tf_op jit(solution)/shard_map/convert_element_type | solution.py:513
  (221 shorter events, 54.7 us)
Async XLA Ops:
  4.3 18.1 %collective-permute-start.5 = (bf16[256,1024]{1,0:T(8,128)(2,1)S(1)}, bf16[256,1024]{1,0:T(8,128)(2,1)}, u32[]{:S(2)}, u32[]{:S(2)}) collective-permute-start(bf16[256,1024]{1,0:T(8,128)(2,1)S(1)} %constant_dynamic-update-slice_fusion), channel_id=1, source_target_pairs={{0,1},{2,3},{5,4},{7,6},{8,9},{10,11},{13,12},{15,14},{16,17},{18,... | collective-permute-start | bytes 1572872 | tf_op jit(solution)/shard_map/ppermute | solution.py:215
  7.6 13.5 %collective-permute-start.8 = (bf16[256,1024]{1,0:T(8,128)(2,1)S(1)}, bf16[256,1024]{1,0:T(8,128)(2,1)}, u32[]{:S(2)}, u32[]{:S(2)}) collective-permute-start(bf16[256,1024]{1,0:T(8,128)(2,1)S(1)} %constant_dynamic-update-slice_fusion), channel_id=1, source_target_pairs={{1,4},{3,6},{4,1},{6,3},{9,12},{11,14},{12,9},{14,11},{17,20},{19,... | collective-permute-start | bytes 1572872 | tf_op jit(solution)/shard_map/ppermute | solution.py:215
  9.0 35.2 %collective-permute-start = (bf16[512,512]{1,0:T(8,128)(2,1)}, bf16[512,512]{1,0:T(8,128)(2,1)S(1)}, u32[]{:S(2)}, u32[]{:S(2)}) collective-permute-start(bf16[512,512]{1,0:T(8,128)(2,1)} %own.1), channel_id=1, source_target_pairs={{0,2},{1,4},{2,0},{3,6},{4,1},{5,7},{6,3},{7,5},{8,10},{9,12},{10,... | collective-permute-start | bytes 1572872 | tf_op jit(solution)/shard_map/ppermute | solution.py:215
  13.2 19.4 %collective-permute-start.20 = (bf16[1024,256]{1,0:T(8,128)(2,1)}, bf16[1024,256]{1,0:T(8,128)(2,1)S(1)}, u32[]{:S(2)}, u32[]{:S(2)}) collective-permute-start(bf16[1024,256]{1,0:T(8,128)(2,1)} %pad_maximum_fusion), channel_id=1, source_target_pairs={{1,4},{3,6},{4,1},{6,3},{9,12},{11,14},{12,9},{14,11},{17,20},{19,... | collective-permute-start | bytes 1572872 | tf_op jit(solution)/shard_map/ppermute | solution.py:215
  15.8 21.4 %collective-permute-start.22 = (bf16[768,256]{1,0:T(8,128)(2,1)S(1)}, bf16[768,256]{1,0:T(8,128)(2,1)S(1)}, u32[]{:S(2)}, u32[]{:S(2)}) collective-permute-start(bf16[768,256]{1,0:T(8,128)(2,1)S(1)} %constant_dynamic-update-slice_fusion.4), channel_id=1, source_target_pairs={{0,1},{2,3},{5,4},{7,6},{8,9},{10,11},{13,12},{15,14},{16,17},{18,... | collective-permute-start | bytes 1179656 | tf_op jit(solution)/shard_map/ppermute | solution.py:215
  22.5 12.9 %collective-permute-start.6 = (bf16[256,1024]{1,0:T(8,128)(2,1)S(1)}, bf16[256,1024]{1,0:T(8,128)(2,1)}, u32[]{:S(2)}, u32[]{:S(2)}) collective-permute-start(bf16[256,1024]{1,0:T(8,128)(2,1)S(1)} %broadcast_select_fusion.1.refs_1_), channel_id=1, source_target_pairs={{0,8},{2,10},{4,12},{6,14},{8,16},{9,1},{10,18},{11,3},{12,20},{13... | collective-permute-start | bytes 1572872 | tf_op jit(solution)/shard_map/ppermute | solution.py:215
  28.1 18.1 %collective-permute-start.10 = (bf16[256,1024]{1,0:T(8,128)(2,1)S(1)}, bf16[256,1024]{1,0:T(8,128)(2,1)}, u32[]{:S(2)}, u32[]{:S(2)}) collective-permute-start(bf16[256,1024]{1,0:T(8,128)(2,1)S(1)} %broadcast_select_fusion.refs_2_), channel_id=1, source_target_pairs={{0,8},{2,10},{4,12},{6,14},{8,16},{9,1},{10,18},{11,3},{12,20},{13... | collective-permute-start | bytes 1572872 | tf_op jit(solution)/shard_map/ppermute | solution.py:215
  34.1 13.7 %collective-permute-start.23 = (bf16[768,256]{1,0:T(8,128)(2,1)}, bf16[768,256]{1,0:T(8,128)(2,1)}, u32[]{:S(2)}, u32[]{:S(2)}) collective-permute-start(bf16[768,256]{1,0:T(8,128)(2,1)} %slice.286), channel_id=1, source_target_pairs={{1,0},{3,2},{4,5},{6,7},{9,8},{11,10},{12,13},{14,15},{17,16},{19,... | collective-permute-start | bytes 1179656 | tf_op jit(solution)/shard_map/ppermute | solution.py:215
  35.4 14.6 %collective-permute-start.7 = (bf16[256,1024]{1,0:T(8,128)(2,1)}, bf16[256,1024]{1,0:T(8,128)(2,1)}, u32[]{:S(2)}, u32[]{:S(2)}) collective-permute-start(bf16[256,1024]{1,0:T(8,128)(2,1)} %collective-permute-done.6.refs_3_), channel_id=1, source_target_pairs={{8,16},{9,0},{10,18},{11,2},{12,20},{13,4},{14,22},{15,6},{16,24},... | collective-permute-start | bytes 1572872 | tf_op jit(solution)/shard_map/ppermute | solution.py:215
  37.2 15.2 %collective-permute-start.1 = (bf16[512,512]{1,0:T(8,128)(2,1)S(1)}, bf16[512,512]{1,0:T(8,128)(2,1)S(1)}, u32[]{:S(2)}, u32[]{:S(2)}) collective-permute-start(bf16[512,512]{1,0:T(8,128)(2,1)S(1)} %copy-done.16), channel_id=1, source_target_pairs={{0,4},{1,2},{2,6},{3,0},{4,7},{5,1},{6,5},{7,3},{8,12},{9,10},{10,... | collective-permute-start | bytes 1572872 | tf_op jit(solution)/shard_map/ppermute | solution.py:215
  44.3 15.5 %collective-permute-start.2 = (bf16[512,512]{1,0:T(8,128)(2,1)S(1)}, bf16[512,512]{1,0:T(8,128)(2,1)S(1)}, u32[]{:S(2)}, u32[]{:S(2)}) collective-permute-start(bf16[512,512]{1,0:T(8,128)(2,1)S(1)} %copy-done.16), channel_id=1, source_target_pairs={{1,0},{3,2},{4,5},{6,7},{9,8},{11,10},{12,13},{14,15},{17,16},{19,... | collective-permute-start | bytes 1572872 | tf_op jit(solution)/shard_map/ppermute | solution.py:215
  46.3 15.6 %collective-permute-start.11 = (bf16[256,1024]{1,0:T(8,128)(2,1)}, bf16[256,1024]{1,0:T(8,128)(2,1)}, u32[]{:S(2)}, u32[]{:S(2)}) collective-permute-start(bf16[256,1024]{1,0:T(8,128)(2,1)} %collective-permute-done.10.refs_4_), channel_id=1, source_target_pairs={{8,17},{9,1},{10,19},{11,3},{12,21},{13,5},{14,23},{15,7},{16,25},... | collective-permute-start | bytes 1572872 | tf_op jit(solution)/shard_map/ppermute | solution.py:215
  47.8 17.8 %collective-permute-start.3 = (bf16[512,512]{1,0:T(8,128)(2,1)S(1)}, bf16[512,512]{1,0:T(8,128)(2,1)}, u32[]{:S(2)}, u32[]{:S(2)}) collective-permute-start(bf16[512,512]{1,0:T(8,128)(2,1)S(1)} %collective-permute-done.p1), channel_id=1, source_target_pairs={{1,3},{3,1},{4,6},{6,4},{9,11},{11,9},{12,14},{14,12},{17,19},{19,... | collective-permute-start | bytes 1572872 | tf_op jit(solution)/shard_map/ppermute | solution.py:215
  50.0 21.9 %collective-permute-start.13 = (bf16[256,1024]{1,0:T(8,128)(2,1)}, bf16[256,1024]{1,0:T(8,128)(2,1)}, u32[]{:S(2)}, u32[]{:S(2)}) collective-permute-start(bf16[256,1024]{1,0:T(8,128)(2,1)} %collective-permute-done.7), channel_id=1, source_target_pairs={{8,0},{10,2},{12,4},{14,6},{16,24},{18,26},{20,28},{22,30}} | collective-permute-start | bytes 1572872 | tf_op jit(solution)/shard_map/ppermute | solution.py:215
  52.4 12.5 %collective-permute-start.24 = (bf16[768,256]{1,0:T(8,128)(2,1)S(1)}, bf16[768,256]{1,0:T(8,128)(2,1)}, u32[]{:S(2)}, u32[]{:S(2)}) collective-permute-start(bf16[768,256]{1,0:T(8,128)(2,1)S(1)} %broadcast_select_fusion.7.refs_0_), channel_id=1, source_target_pairs={{0,8},{2,10},{4,12},{6,14},{8,16},{9,1},{10,18},{11,3},{12,20},{13... | collective-permute-start | bytes 1179656 | tf_op jit(solution)/shard_map/ppermute | solution.py:215
  61.8 12.6 %collective-permute-start.14 = (bf16[256,1024]{1,0:T(8,128)(2,1)}, bf16[256,1024]{1,0:T(8,128)(2,1)}, u32[]{:S(2)}, u32[]{:S(2)}) collective-permute-start(bf16[256,1024]{1,0:T(8,128)(2,1)} %collective-permute-done.11), channel_id=1, source_target_pairs={{9,1},{11,3},{13,5},{15,7},{17,25},{19,27},{21,29},{23,31}} | collective-permute-start | bytes 1572872 | tf_op jit(solution)/shard_map/ppermute | solution.py:215
  64.9 19.5 %collective-permute-start.4 = (bf16[512,512]{1,0:T(8,128)(2,1)}, bf16[512,512]{1,0:T(8,128)(2,1)S(1)}, u32[]{:S(2)}, u32[]{:S(2)}) collective-permute-start(bf16[512,512]{1,0:T(8,128)(2,1)} %copy-done.18), channel_id=1, source_target_pairs={{1,3},{3,1},{4,6},{6,4},{9,11},{11,9},{12,14},{14,12},{17,19},{19,... | collective-permute-start | bytes 1572872 | tf_op jit(solution)/shard_map/ppermute | solution.py:215
  65.6 16.1 %collective-permute-start.28 = (bf16[768,256]{1,0:T(8,128)(2,1)}, bf16[768,256]{1,0:T(8,128)(2,1)}, u32[]{:S(2)}, u32[]{:S(2)}) collective-permute-start(bf16[768,256]{1,0:T(8,128)(2,1)} %collective-permute-done.24.refs_2_), channel_id=1, source_target_pairs={{8,16},{9,0},{10,18},{11,2},{12,20},{13,4},{14,22},{15,6},{16,24},... | collective-permute-start | bytes 1179656 | tf_op jit(solution)/shard_map/ppermute | solution.py:215
  68.5 18.7 %collective-permute-start.16 = (bf16[256,1024]{1,0:T(8,128)(2,1)}, bf16[256,1024]{1,0:T(8,128)(2,1)}, u32[]{:S(2)}, u32[]{:S(2)}) collective-permute-start(bf16[256,1024]{1,0:T(8,128)(2,1)} %collective-permute-done.6.refs_3_), channel_id=1, source_target_pairs={{0,1},{1,0},{2,3},{3,2},{4,5},{5,4},{6,7},{7,6},{8,9},{9,8},{10,11... | collective-permute-start | bytes 1572872 | tf_op jit(solution)/shard_map/ppermute | solution.py:215
  74.4 20.3 %collective-permute-start.17 = (bf16[256,1024]{1,0:T(8,128)(2,1)}, bf16[256,1024]{1,0:T(8,128)(2,1)}, u32[]{:S(2)}, u32[]{:S(2)}) collective-permute-start(bf16[256,1024]{1,0:T(8,128)(2,1)} %collective-permute-done.10.refs_4_), channel_id=1, source_target_pairs={{0,1},{1,0},{2,3},{3,2},{4,5},{5,4},{6,7},{7,6},{8,9},{9,8},{10,11... | collective-permute-start | bytes 1572872 | tf_op jit(solution)/shard_map/ppermute | solution.py:215
  81.7 19.2 %collective-permute-start.31 = (bf16[768,256]{1,0:T(8,128)(2,1)}, bf16[768,256]{1,0:T(8,128)(2,1)}, u32[]{:S(2)}, u32[]{:S(2)}) collective-permute-start(bf16[768,256]{1,0:T(8,128)(2,1)} %collective-permute-done.28), channel_id=1, source_target_pairs={{8,0},{10,2},{12,4},{14,6},{16,24},{18,26},{20,28},{22,30}} | collective-permute-start | bytes 1179656 | tf_op jit(solution)/shard_map/ppermute | solution.py:215
  83.0 18.1 %collective-permute-start.32 = (bf16[768,256]{1,0:T(8,128)(2,1)}, bf16[768,256]{1,0:T(8,128)(2,1)}, u32[]{:S(2)}, u32[]{:S(2)}) collective-permute-start(bf16[768,256]{1,0:T(8,128)(2,1)} %collective-permute-done.29), channel_id=1, source_target_pairs={{9,1},{11,3},{13,5},{15,7},{17,25},{19,27},{21,29},{23,31}} | collective-permute-start | bytes 1179656 | tf_op jit(solution)/shard_map/ppermute | solution.py:215
  84.4 18.1 %collective-permute-start.12 = (bf16[256,1024]{1,0:T(8,128)(2,1)S(1)}, bf16[256,1024]{1,0:T(8,128)(2,1)S(1)}, u32[]{:S(2)}, u32[]{:S(2)}) collective-permute-start(bf16[256,1024]{1,0:T(8,128)(2,1)S(1)} %broadcast_select_fusion.3.refs_1_), channel_id=1, source_target_pairs={{0,1},{1,0},{2,3},{3,2},{4,5},{5,4},{6,7},{7,6},{8,9},{9,8},{10,11... | collective-permute-start | bytes 1572872 | tf_op jit(solution)/shard_map/ppermute | solution.py:215
  87.1 15.4 %collective-permute-start.15 = (bf16[256,1024]{1,0:T(8,128)(2,1)S(1)}, bf16[256,1024]{1,0:T(8,128)(2,1)}, u32[]{:S(2)}, u32[]{:S(2)}) collective-permute-start(bf16[256,1024]{1,0:T(8,128)(2,1)S(1)} %broadcast_select_fusion.2.refs_3_), channel_id=1, source_target_pairs={{0,1},{1,0},{2,3},{3,2},{4,5},{5,4},{6,7},{7,6},{8,9},{9,8},{10,11... | collective-permute-start | bytes 1572872 | tf_op jit(solution)/shard_map/ppermute | solution.py:215
  94.8 51.2 %collective-permute-start.26 = (bf16[768,256]{1,0:T(8,128)(2,1)}, bf16[768,256]{1,0:T(8,128)(2,1)}, u32[]{:S(2)}, u32[]{:S(2)}) collective-permute-start(bf16[768,256]{1,0:T(8,128)(2,1)} %collective-permute-done.24.refs_2_), channel_id=1, source_target_pairs={{0,1},{1,0},{2,3},{3,2},{4,5},{5,4},{6,7},{7,6},{8,9},{9,8},{10,11... | collective-permute-start | bytes 1179656 | tf_op jit(solution)/shard_map/ppermute | solution.py:215
  100.9 45.1 %collective-permute-start.27 = (bf16[768,256]{1,0:T(8,128)(2,1)}, bf16[768,256]{1,0:T(8,128)(2,1)}, u32[]{:S(2)}, u32[]{:S(2)}) collective-permute-start(bf16[768,256]{1,0:T(8,128)(2,1)} %collective-permute-done.25.refs_3_), channel_id=1, source_target_pairs={{0,1},{1,0},{2,3},{3,2},{4,5},{5,4},{6,7},{7,6},{8,9},{9,8},{10,11... | collective-permute-start | bytes 1179656 | tf_op jit(solution)/shard_map/ppermute | solution.py:215
  101.1 44.9 %collective-permute-start.30 = (bf16[768,256]{1,0:T(8,128)(2,1)}, bf16[768,256]{1,0:T(8,128)(2,1)}, u32[]{:S(2)}, u32[]{:S(2)}) collective-permute-start(bf16[768,256]{1,0:T(8,128)(2,1)} %broadcast_select_fusion.5.refs_6_), channel_id=1, source_target_pairs={{0,1},{1,0},{2,3},{3,2},{4,5},{5,4},{6,7},{7,6},{8,9},{9,8},{10,11... | collective-permute-start | bytes 1179656 | tf_op jit(solution)/shard_map/ppermute | solution.py:215
  117.7 28.3 %collective-permute-start.33 = (bf16[768,256]{1,0:T(8,128)(2,1)S(1)}, bf16[768,256]{1,0:T(8,128)(2,1)S(1)}, u32[]{:S(2)}, u32[]{:S(2)}) collective-permute-start(bf16[768,256]{1,0:T(8,128)(2,1)S(1)} %broadcast_select_fusion.4.refs_8_), channel_id=1, source_target_pairs={{0,1},{1,0},{2,3},{3,2},{4,5},{5,4},{6,7},{7,6},{8,9},{9,8},{10,11... | collective-permute-start | bytes 1179656 | tf_op jit(solution)/shard_map/ppermute | solution.py:215
  156.1 15.6 %collective-permute-start.37 = (bf16[512,512]{1,0:T(8,128)(2,1)}, bf16[512,512]{1,0:T(8,128)(2,1)S(1)}, u32[]{:S(2)}, u32[]{:S(2)}) collective-permute-start(bf16[512,512]{1,0:T(8,128)(2,1)} %get-tuple-element.9), channel_id=1, source_target_pairs={{0,3},{1,7},{2,1},{3,5},{4,2},{5,6},{6,0},{7,4},{8,11},{9,15},{10,... | collective-permute-start | bytes 1572872 | tf_op jit(solution)/shard_map/ppermute | solution.py:215
  158.6 24.3 %collective-permute-start.36 = (bf16[512,512]{1,0:T(8,128)(2,1)}, bf16[512,512]{1,0:T(8,128)(2,1)S(1)}, u32[]{:S(2)}, u32[]{:S(2)}) collective-permute-start(bf16[512,512]{1,0:T(8,128)(2,1)} %get-tuple-element.8), channel_id=1, source_target_pairs={{0,2},{1,6},{2,0},{3,4},{4,3},{5,7},{6,1},{7,5},{8,10},{9,14},{10,... | collective-permute-start | bytes 1572872 | tf_op jit(solution)/shard_map/ppermute | solution.py:215
  159.1 23.8 %collective-permute-start.35 = (bf16[512,512]{1,0:T(8,128)(2,1)}, bf16[512,512]{1,0:T(8,128)(2,1)S(1)}, u32[]{:S(2)}, u32[]{:S(2)}) collective-permute-start(bf16[512,512]{1,0:T(8,128)(2,1)} %get-tuple-element.7), channel_id=1, source_target_pairs={{0,1},{1,5},{2,3},{3,7},{4,0},{5,4},{6,2},{7,6},{8,9},{9,13},{10,1... | collective-permute-start | bytes 1572872 | tf_op jit(solution)/shard_map/ppermute | solution.py:215
  159.7 23.2 %collective-permute-start.34 = (bf16[512,512]{1,0:T(8,128)(2,1)}, bf16[512,512]{1,0:T(8,128)(2,1)S(1)}, u32[]{:S(2)}, u32[]{:S(2)}) collective-permute-start(bf16[512,512]{1,0:T(8,128)(2,1)} %get-tuple-element.6), channel_id=1, source_target_pairs={{1,4},{3,6},{4,1},{6,3},{9,12},{11,14},{12,9},{14,11},{17,20},{19,... | collective-permute-start | bytes 1572872 | tf_op jit(solution)/shard_map/ppermute | solution.py:215
  (54 other events, 620.3 us)

commit v2 on v0

--- a/solution.py
+++ b/solution.py
@@ -1,6 +1,10 @@
+import functools
+
 import jax
 import jax.numpy as jnp
 from jax import lax
+from jax.experimental import pallas as pl
+from jax.experimental.pallas import tpu as pltpu
 from jax.sharding import PartitionSpec as P
 
 HD = 64
@@ -99,6 +103,38 @@
     weights = (exps / row_total[..., None]).astype(jnp.bfloat16)
     attended = jnp.einsum("hgqk,khd->qhgd", weights, values, preferred_element_type=jnp.float32)
     return (attended.astype(jnp.bfloat16), row_top + jnp.log(row_total))
+
+
+def attend_all(rot_query, key_ext, value_ext, sink_logit, offset, seq_total):
+    tok_rows = rot_query.shape[0]
+    heads_local = rot_query.shape[1] // HD
+    kv_local = key_ext.shape[1] // HD
+    grp = heads_local // kv_local
+    query_heads = rot_query.reshape(tok_rows, kv_local, grp, HD)
+    key_heads = key_ext.reshape(-1, kv_local, HD)
+    value_heads = value_ext.reshape(-1, kv_local, HD)
+    sink = sink_logit.reshape(kv_local, grp)
+    block_rows = min(tok_rows, 256)
+    attended_parts = []
+    log_parts = []
+    for block_index in range(tok_rows // block_rows):
+        start = block_index * block_rows
+        query_pos = offset + start + jnp.arange(block_rows, dtype=jnp.int32)
+        key_pos = offset + start - WINDOW + jnp.arange(block_rows + 2 * WINDOW, dtype=jnp.int32)
+        attended_block, log_block = attend_block(
+            query_heads[start : start + block_rows],
+            key_heads[start : start + block_rows + 2 * WINDOW],
+            value_heads[start : start + block_rows + 2 * WINDOW],
+            sink,
+            query_pos,
+            key_pos,
+            seq_total,
+        )
+        attended_parts.append(attended_block.reshape(block_rows, heads_local * HD))
+        log_parts.append(log_block.reshape(heads_local, block_rows))
+    attended = jnp.concatenate(attended_parts, 0)
+    log_weight = jnp.concatenate(log_parts, 1)
+    return (attended, log_weight)
 
 
 def fetch_outputs(out_pool_weight, out_attn_weight):
@@ -151,33 +187,7 @@
     pool_out = jnp.dot(pooled, pool_mix_weight[0], preferred_element_type=jnp.float32).astype(
         jnp.bfloat16
     )
-    heads_local = rot_query.shape[1] // HD
-    kv_local = key_width // HD
-    grp = heads_local // kv_local
-    query_heads = rot_query.reshape(tok_rows, kv_local, grp, HD)
-    key_heads = key_ext.reshape(-1, kv_local, HD)
-    value_heads = value_ext.reshape(-1, kv_local, HD)
-    sink = sink_logit.reshape(kv_local, grp)
-    block_rows = min(tok_rows, 256)
-    attended_parts = []
-    log_parts = []
-    for block_index in range(tok_rows // block_rows):
-        start = block_index * block_rows
-        query_pos = offset + start + jnp.arange(block_rows, dtype=jnp.int32)
-        key_pos = offset + start - WINDOW + jnp.arange(block_rows + 2 * WINDOW, dtype=jnp.int32)
-        attended_block, log_block = attend_block(
-            query_heads[start : start + block_rows],
-            key_heads[start : start + block_rows + 2 * WINDOW],
-            value_heads[start : start + block_rows + 2 * WINDOW],
-            sink,
-            query_pos,
-            key_pos,
-            seq_total,
-        )
-        attended_parts.append(attended_block.reshape(block_rows, heads_local * HD))
-        log_parts.append(log_block.reshape(heads_local, block_rows))
-    attended = jnp.concatenate(attended_parts, 0)
-    log_weight = jnp.concatenate(log_parts, 1)
+    attended, log_weight = attend_all(rot_query, key_ext, value_ext, sink_logit, offset, seq_total)
     out_pool_full, out_attn_full = fetch_outputs(out_pool_weight, out_attn_weight)
     term = jnp.dot(pool_out, out_pool_full, preferred_element_type=jnp.float32)
     term = term + jnp.dot(attended, out_attn_full, preferred_element_type=jnp.float32)
@@ -185,9 +195,652 @@
     return (mixed, log_weight)
 
 
+ANY = pl.BlockSpec(memory_space=pl.ANY)
+SMEM = pl.BlockSpec(memory_space=pltpu.SMEM)
+VMEM = pl.BlockSpec(memory_space=pltpu.VMEM)
+
+
+def lin(z, y, x, c):
+    return ((z * 2 + y) * 2 + x) * 2 + c
+
+
+def make_perm(rule):
+    pairs = []
+    for z in range(4):
+        for y in range(2):
+            for x in range(2):
+                for c in range(2):
+                    to = rule(z, y, x, c)
+                    if to is not None and to != (z, y, x, c):
+                        pairs.append((lin(z, y, x, c), lin(*to)))
+    return pairs
+
+
+def send(name, value, rule):
+    with jax.named_scope(name):
+        return lax.ppermute(value, ("sp", "tp"), make_perm(rule))
+
+
+def after(value, *tokens):
+    return lax.optimization_barrier((value, *tokens))[0]
+
+
+def swap_away(z, y, x, c):
+    return (z, c, x, y) if y != c else None
+
+
+def home_to_away(z, y, x, c):
+    return (z, y, x, 1 - c) if y == c else None
+
+
+def away_to_home(z, y, x, c):
+    return (z, y, x, 1 - c) if y != c else None
+
+
+def other_core(z, y, x, c):
+    return (z, y, x, 1 - c)
+
+
+def from_core(core):
+    return lambda z, y, x, c: (z, y, x, 1 - c) if c == core else None
+
+
+def line_one(z, y, x, c):
+    if c == 0:
+        return (z + 1, y, x, c) if z < 3 else None
+    return (z - 1, y, x, c) if z > 0 else None
+
+
+def line_two(core):
+    def rule(z, y, x, c):
+        if z not in (1, 2):
+            return None
+        return (z + 1 if c == 0 else z - 1, y, x, core)
+
+    return rule
+
+
+def line_three(core):
+    def rule(z, y, x, c):
+        if c != core or z not in (1, 2):
+            return None
+        return (0 if z == 1 else 3, y, x, c)
+
+    return rule
+
+
+def end_core(core):
+    return lambda z, y, x, c: (z, y, x, 1 - c) if c == core and z in (0, 3) else None
+
+
+def token_one(z, y, x, c):
+    return (z, y, 1 - x, c) if y == c else (z, 1 - y, x, 1 - c)
+
+
+def token_two(z, y, x, c):
+    return (z, y, 1 - x, 1 - c) if y != c else (z, 1 - y, x, c)
+
+
+def token_diag(z, y, x, c):
+    return (z, y, 1 - x, c) if y != c else None
+
+
+def halo_next(z, y, x, c):
+    if c == 0:
+        return (z, y, x, 1)
+    return (z + 1, y, x, 0) if z < 3 else None
+
+
+def halo_prev(z, y, x, c):
+    if c == 1:
+        return (z, y, x, 0)
+    return (z - 1, y, x, 1) if z > 0 else None
+
+
+def late_block(z):
+    return 3 if z < 2 else 0
+
+
+def part_early(r):
+    def rule(z, y, x, c):
+        j = (2 * x + y) ^ r
+        return None if j == late_block(z) else (z, c, j // 2, j % 2)
+
+    return rule
+
+
+def part_late(r):
+    def rule(z, y, x, c):
+        j = (2 * x + y) ^ r
+        return (z, c, j // 2, j % 2) if j == late_block(z) else None
+
+    return rule
+
+
+def pack_kernel(axis, *refs):
+    sources, out, sems = refs[:-2], refs[-2], refs[-1]
+    copies = []
+    at = 0
+    for i, source in enumerate(sources):
+        size = source.shape[axis]
+        span = pl.ds(at, size)
+        where = (span, slice(None)) if axis == 0 else (slice(None), span)
+        copies.append(pltpu.make_async_copy(source, out.at[where], sems.at[i]))
+        copies[-1].start()
+        at += size
+    for copy in copies:
+        copy.wait()
+
+
+def pack(name, arrays, axis):
+    shape = list(arrays[0].shape)
+    shape[axis] = sum(a.shape[axis] for a in arrays)
+    return pl.pallas_call(
+        functools.partial(pack_kernel, axis),
+        out_shape=jax.ShapeDtypeStruct(tuple(shape), arrays[0].dtype),
+        in_specs=[ANY] * len(arrays),
+        out_specs=ANY,
+        scratch_shapes=[pltpu.SemaphoreType.DMA((len(arrays),))],
+        name=name,
+    )(*arrays)
+
+
+def fetch(slots, buf, sems):
+    for i, choices in enumerate(slots):
+        for when, ref in choices:
+            copy = pltpu.make_async_copy(ref, buf.at[i], sems.at[i])
+            if when is None:
+                copy.start()
+            else:
+                pl.when(when)(copy.start)
+
+
+def arrived(slots, buf, sems, i):
+    pltpu.make_async_copy(slots[i][0][1], buf.at[i], sems.at[i]).wait()
+
+
+def norm_kernel(idx, own, p1, p2, p3, p4, p5, gain, out, buf, sems):
+    home = idx[0]
+    at_home = (own, p3, p1, p2)
+    at_away = (p2, p1, p5, p4)
+    for i in range(4):
+        for when, ref in ((home == 1, at_home[i]), (home == 0, at_away[i])):
+            pl.when(when)(pltpu.make_async_copy(ref, buf.at[idx[1 + i]], sems.at[i]).start)
+    for i in range(4):
+        pltpu.make_async_copy(own, buf.at[idx[1 + i]], sems.at[i]).wait()
+    blocks, rows, wide = buf.shape
+    half = wide // 2
+    step = 64
+
+    def body(i, carry):
+        at = pl.ds(pl.multiple_of(i * step, step), step)
+        total = jnp.zeros((step, wide), jnp.float32)
+        for b in range(blocks):
+            v = buf[b, at, :].astype(jnp.float32)
+            total = total + v * v
+        scale = lax.rsqrt(jnp.sum(total, -1, keepdims=True) / (blocks * wide) + norm_eps)
+        for b in range(blocks):
+            v = buf[b, at, :].astype(jnp.float32)
+            v = (v * scale * gain[:, b * wide : (b + 1) * wide]).astype(jnp.bfloat16)
+            out[2 * b, at, :] = v[:, :half]
+            out[2 * b + 1, at, :] = v[:, half:]
+        return carry
+
+    lax.fori_loop(0, rows // step, body, 0)
+
+
+def norm_tokens(idx, pieces, gain):
+    rows, wide = pieces[0].shape
+    return pl.pallas_call(
+        norm_kernel,
+        out_shape=jax.ShapeDtypeStruct((8, rows, wide // 2), jnp.bfloat16),
+        in_specs=[SMEM] + [ANY] * 6 + [VMEM],
+        out_specs=VMEM,
+        scratch_shapes=[pltpu.VMEM((4, rows, wide), jnp.bfloat16), pltpu.SemaphoreType.DMA((4,))],
+        name="norm",
+    )(idx, *pieces, gain)
+
+
+def near_kernel(idx, normed, near, far, d1, s1, ed1, es1, out, buf, sems):
+    slots = [[(None, ref)] for ref in (near, far, d1, s1, ed1, es1)]
+    fetch(slots, buf, sems)
+    for pair in range(3):
+        arrived(slots, buf, sems, 2 * pair)
+        arrived(slots, buf, sems, 2 * pair + 1)
+
+        def add():
+            rows = normed.shape[1]
+            for at in range(0, rows, rows // 2):
+                span = pl.ds(at, rows // 2)
+                part = jnp.dot(normed[idx[2 * pair], span, :], buf[2 * pair], preferred_element_type=jnp.float32)
+                part += jnp.dot(normed[idx[2 * pair + 1], span, :], buf[2 * pair + 1], preferred_element_type=jnp.float32)
+                if pair == 0:
+                    out[span, :] = part
+                else:
+                    out[span, :] += part
+
+        if pair == 0:
+            add()
+        else:
+            pl.when(idx[2 * pair] >= 0)(add)
+
+
+def project_near(idx, normed, slots):
+    rows = normed.shape[1]
+    deep, cols = slots[0].shape
+    return pl.pallas_call(
+        near_kernel,
+        out_shape=jax.ShapeDtypeStruct((rows, cols), jnp.float32),
+        in_specs=[SMEM, VMEM] + [ANY] * 6,
+        out_specs=VMEM,
+        scratch_shapes=[pltpu.VMEM((6, deep, cols), jnp.bfloat16), pltpu.SemaphoreType.DMA((6,))],
+        name="project_near",
+    )(idx, normed, *slots)
+
+
+def turn(v, cosine, sine):
+    lane = lax.broadcasted_iota(jnp.int32, v.shape, 1)
+    quarter = HD // 4
+    partner = jnp.where(lane % (2 * quarter) < quarter, pltpu.roll(v, v.shape[1] - quarter, 1), pltpu.roll(v, quarter, 1))
+    return v * cosine + partner * sine
+
+
+def far_kernel(widths, idx, normed, acc, cosine, sine, *refs):
+    d2, s2, ed2, es2, d3, s3, ed3, es3, query, pair, pool, low, high, buf, sems = refs
+    core = idx[0]
+    slots = [[(core == 0, a), (core == 1, b)] for a, b in ((d2, ed2), (es2, s2), (d3, ed3), (es3, s3))]
+    fetch(slots, buf, sems)
+    for i in range(4):
+        arrived(slots, buf, sems, i)
+    rows = normed.shape[1]
+    q_w, kv_w = widths
+    half = rows // 2
+    for at in range(0, rows, half):
+        span = pl.ds(at, half)
+        total = acc[span, :]
+        for i in range(4):
+            total += jnp.dot(normed[idx[1 + i], span, :], buf[i], preferred_element_type=jnp.float32)
+        total = total.astype(jnp.bfloat16)
+        co, si = cosine[span, :], sine[span, :]
+        lanes = co.shape[1]
+        for col in range(0, q_w + kv_w, lanes):
+            v = turn(total[:, col : col + lanes].astype(jnp.float32), co, si).astype(jnp.bfloat16)
+            if col < q_w:
+                query[span, col : col + lanes] = v
+            else:
+                pair[span, col - q_w : col - q_w + lanes] = v
+        pair[span, kv_w:] = total[:, q_w + kv_w : q_w + 2 * kv_w]
+        pool[span, :] = total[:, q_w + 2 * kv_w :]
+    low[:WINDOW, :] = pair[:WINDOW, :]
+    low[WINDOW:, :] = pool[:pool_reach, :]
+    high[:WINDOW, :] = pair[rows - WINDOW :, :]
+    high[WINDOW:, :] = pool[rows - pool_reach :, :]
+
+
+def project_far(idx, normed, acc, tables, slots, widths):
+    rows = normed.shape[1]
+    deep, cols = slots[0].shape
+    q_w, kv_w = widths
+    pool_w = cols - q_w - 2 * kv_w
+    edge = (WINDOW + pool_reach, pool_w)
+    return pl.pallas_call(
+        functools.partial(far_kernel, widths),
+        out_shape=[
+            jax.ShapeDtypeStruct(shape, jnp.bfloat16)
+            for shape in ((rows, q_w), (rows, 2 * kv_w), (rows, pool_w), edge, edge)
+        ],
+        in_specs=[SMEM] + [VMEM] * 4 + [ANY] * 8,
+        out_specs=[VMEM] * 5,
+        scratch_shapes=[pltpu.VMEM((4, deep, cols), jnp.bfloat16), pltpu.SemaphoreType.DMA((4,))],
+        name="project_far",
+    )(idx, normed, acc, *tables, *slots)
+
+
+def pool_kernel(seq_total, idx, own, before, behind, mix, out, ext):
+    rows, wide = own.shape
+    ext[:pool_reach, :] = before[WINDOW:, :].astype(jnp.float32)
+    ext[pool_reach : pool_reach + rows, :] = own[...].astype(jnp.float32)
+    ext[pool_reach + rows :, :] = behind[WINDOW:, :].astype(jnp.float32)
+    group, offset = idx[0], idx[1]
+    position = offset + lax.broadcasted_iota(jnp.int32, (rows, 1), 0)
+    for g in range(4):
+
+        @pl.when(group == g)
+        def _():
+            reach = 1 << g
+            total = ext[pool_reach - reach : pool_reach - reach + rows, :]
+            for shift in range(1 - reach, reach):
+                total = total + ext[pool_reach + shift : pool_reach + shift + rows, :]
+            count = jnp.minimum(position + reach, seq_total) - jnp.maximum(position - reach, 0)
+            mean = total / count.astype(jnp.float32)
+            pooled = (mean - ext[pool_reach : pool_reach + rows, :]).astype(jnp.bfloat16)
+            out[...] = jnp.dot(pooled, mix[...], preferred_element_type=jnp.float32).astype(jnp.bfloat16)
+
+
+def pool_mixer(idx, own, before, behind, mix, seq_total):
+    rows, wide = own.shape
+    return pl.pallas_call(
+        functools.partial(pool_kernel, seq_total),
+        out_shape=jax.ShapeDtypeStruct((rows, mix.shape[1]), jnp.bfloat16),
+        in_specs=[SMEM] + [VMEM] * 4,
+        out_specs=VMEM,
+        scratch_shapes=[pltpu.VMEM((rows + 2 * pool_reach, wide), jnp.float32)],
+        name="pool",
+    )(idx, own, before, behind, mix)
+
+
+def attend_kernel(seq_total, idx, query, pair, before, behind, sink, out, logs, keys, values):
+    rows = query.shape[0]
+    lanes = 2 * HD
+    block = WINDOW
+    span = 3 * block
+    kv_w = pair.shape[1] // 2
+    for ref, col in ((keys, 0), (values, kv_w)):
+        whole = jnp.concatenate(
+            [before[:WINDOW, col : col + kv_w], pair[:, col : col + kv_w], behind[:WINDOW, col : col + kv_w]], 0
+        ).astype(jnp.float32)
+        lane = lax.broadcasted_iota(jnp.int32, whole.shape, 1)
+        turned = pltpu.roll(whole, HD, 1)
+        zero = jnp.zeros_like(whole)
+        ref[0] = jnp.where(lane < HD, whole, zero).astype(jnp.bfloat16)
+        ref[1] = jnp.where(lane >= HD, turned, zero).astype(jnp.bfloat16)
+        ref[2] = jnp.where(lane < HD, turned, zero).astype(jnp.bfloat16)
+        ref[3] = jnp.where(lane >= HD, whole, zero).astype(jnp.bfloat16)
+    pairs = query.shape[1] // lanes
+    per_kv = pairs // 2
+
+    def body(i, carry):
+        start = pl.multiple_of(i * block, block)
+        q_at = lax.broadcasted_iota(jnp.int32, (block, span), 0)
+        k_at = lax.broadcasted_iota(jnp.int32, (block, span), 1)
+        position = idx[1] + start - WINDOW + k_at
+        gap = k_at - q_at
+        valid = (gap >= 0) & (gap <= 2 * WINDOW) & (position >= 0) & (position < seq_total)
+        lane = lax.broadcasted_iota(jnp.int32, (block, lanes), 1)
+        tops = jnp.zeros((block, lanes), jnp.float32)
+        for kv in range(2):
+            for p in range(per_kv):
+                at = kv * per_kv + p
+                q = query[pl.ds(start, block), at * lanes : (at + 1) * lanes]
+                mixed = jnp.zeros((block, lanes), jnp.float32)
+                shares = []
+                for side in range(2):
+                    k = keys[2 * kv + side, pl.ds(start, span), :]
+                    v = values[2 * kv + side, pl.ds(start, span), :]
+                    scores = lax.dot_general(q, k, (((1,), (1,)), ((), ())), preferred_element_type=jnp.float32)
+                    scores = jnp.where(valid, scores * HD ** (-0.5), neg_fill)
+                    head = 2 * at + side
+                    floor = sink[head]
+                    top = jnp.maximum(jnp.max(scores, -1, keepdims=True), floor)
+                    exps = jnp.exp(scores - top)
+                    total = jnp.sum(exps, -1, keepdims=True) + jnp.exp(floor - top)
+                    mixed += jnp.dot(exps.astype(jnp.bfloat16), v, preferred_element_type=jnp.float32)
+                    shares.append(total)
+                    tops = jnp.where(lane == head, top + jnp.log(total), tops)
+                total = jnp.where(lane < HD, shares[0], shares[1])
+                out[pl.ds(start, block), at * lanes : (at + 1) * lanes] = (mixed / total).astype(jnp.bfloat16)
+        logs[:, pl.ds(start, block)] = tops.T[: logs.shape[0], :]
+        return carry
+
+    lax.fori_loop(0, rows // block, body, 0)
+
+
+def attend(idx, query, pair, before, behind, sink, seq_total):
+    rows = query.shape[0]
+    wide = pair.shape[1] // 2
+    return pl.pallas_call(
+        functools.partial(attend_kernel, seq_total),
+        out_shape=[
+            jax.ShapeDtypeStruct(query.shape, jnp.bfloat16),
+            jax.ShapeDtypeStruct((query.shape[1] // HD, rows), jnp.float32),
+        ],
+        in_specs=[SMEM] + [VMEM] * 4 + [SMEM],
+        out_specs=[VMEM] * 2,
+        scratch_shapes=[pltpu.VMEM((4, rows + 2 * WINDOW, wide), jnp.bfloat16)] * 2,
+        name="attend",
+    )(idx, query, pair, before, behind, sink)
+
+
+def early_kernel(idx, pooled, attended, *refs):
+    near, far, d1, s1, ed1, es1, d2, s2, ed2, es2 = refs[:10]
+    outs, buf, sems = refs[10:14], refs[14], refs[15]
+    core = idx[0]
+    slots = [[(None, ref)] for ref in (near, far, d1, s1, ed1, es1)]
+    slots += [[(core == 0, a), (core == 1, b)] for a, b in ((d2, ed2), (es2, s2))]
+    fetch(slots, buf, sems)
+    cut = pooled.shape[1]
+    half = buf.shape[2]
+    for i in range(8):
+        arrived(slots, buf, sems, i)
+        place = idx[1 + i]
+
+        @pl.when(place >= 0)
+        def _():
+            part = jnp.dot(pooled[...], buf[i, :cut, :], preferred_element_type=jnp.float32)
+            part += jnp.dot(attended[...], buf[i, cut:, :], preferred_element_type=jnp.float32)
+            part = part.astype(jnp.bfloat16)
+            col = pl.multiple_of((place % 2) * half, half)
+            for r in range(4):
+
+                @pl.when(place // 2 == r)
+                def _():
+                    outs[r][:, pl.ds(col, half)] = part
+
+
+def out_early(idx, pooled, attended, slots):
+    rows = pooled.shape[0]
+    deep, wide = slots[0].shape
+    return pl.pallas_call(
+        early_kernel,
+        out_shape=[jax.ShapeDtypeStruct((rows, 2 * wide), jnp.bfloat16)] * 4,
+        in_specs=[SMEM] + [VMEM] * 2 + [ANY] * 10,
+        out_specs=[VMEM] * 4,
+        scratch_shapes=[pltpu.VMEM((8, deep, wide), jnp.bfloat16), pltpu.SemaphoreType.DMA((8,))],
+        name="out_early",
+    )(idx, pooled, attended, *slots)
+
+
+def late_kernel(idx, pooled, attended, *refs):
+    d2, s2, ed2, es2, d3, s3, ed3, es3, out, buf, sems = refs
+    core, outer = idx[0], idx[1]
+    slots = []
+    for (a, b), (e, f) in (((d2, ed2), (d3, ed3)), ((es2, s2), (es3, s3))):
+        slots.append(
+            [
+                ((outer == 0) & (core == 0), a),
+                ((outer == 0) & (core == 1), b),
+                ((outer == 1) & (core == 0), e),
+                ((outer == 1) & (core == 1), f),
+            ]
+        )
+    fetch(slots, buf, sems)
+    cut = pooled.shape[1]
+    half = buf.shape[2]
+    for i in range(2):
+        arrived(slots, buf, sems, i)
+        part = jnp.dot(pooled[...], buf[i, :cut, :], preferred_element_type=jnp.float32)
+        part += jnp.dot(attended[...], buf[i, cut:, :], preferred_element_type=jnp.float32)
+        col = pl.multiple_of(idx[2 + i] * half, half)
+        out[:, pl.ds(col, half)] = part.astype(jnp.bfloat16)
+
+
+def out_late(idx, pooled, attended, slots):
+    rows = pooled.shape[0]
+    deep, wide = slots[0].shape
+    return pl.pallas_call(
+        late_kernel,
+        out_shape=jax.ShapeDtypeStruct((rows, 2 * wide), jnp.bfloat16),
+        in_specs=[SMEM] + [VMEM] * 2 + [ANY] * 8,
+        out_specs=VMEM,
+        scratch_shapes=[pltpu.VMEM((2, deep, wide), jnp.bfloat16), pltpu.SemaphoreType.DMA((2,))],
+        name="out_late",
+    )(idx, pooled, attended, *slots)
+
+
+def sum_kernel(idx, *refs):
+    early, late, own_early, own_late, out, buf, sems = refs[:4], refs[4:8], refs[8], refs[9], *refs[10:]
+    is_late, has_own, own_round = idx[0], idx[1], idx[2]
+    slots = []
+    for r in range(4):
+        mine = (has_own == 1) & (own_round == r)
+        slots.append(
+            [
+                ((is_late == 0) & jnp.logical_not(mine), early[r]),
+                ((is_late == 0) & mine, own_early),
+                ((is_late == 1) & jnp.logical_not(mine), late[r]),
+                ((is_late == 1) & mine, own_late),
+            ]
+        )
+    fetch(slots, buf, sems)
+    for r in range(4):
+        arrived(slots, buf, sems, r)
+    total = buf[0].astype(jnp.float32)
+    for r in range(1, 4):
+        total = total + buf[r].astype(jnp.float32)
+    out[...] = total.astype(jnp.bfloat16)
+
+
+def sum_parts(idx, early, late, own_early, own_late):
+    shape = own_late.shape
+    return pl.pallas_call(
+        sum_kernel,
+        out_shape=jax.ShapeDtypeStruct(shape, jnp.bfloat16),
+        in_specs=[SMEM] + [ANY] * 10,
+        out_specs=VMEM,
+        scratch_shapes=[pltpu.VMEM((4, *shape), jnp.bfloat16), pltpu.SemaphoreType.DMA((4,))],
+        name="sum",
+    )(idx, *early, *late, own_early, own_late)
+
+
+def line_gather(name, near, far):
+    d1 = send(name + "_d1", near, line_one)
+    s1 = send(name + "_s1", far, line_one)
+    d2 = send(name + "_d2", d1, line_two(0))
+    s2 = send(name + "_s2", s1, line_two(1))
+    d3 = send(name + "_d3", d2, line_three(0))
+    s3 = send(name + "_s3", s2, line_three(1))
+    ed1 = send(name + "_ed1", d1, other_core)
+    es1 = send(name + "_es1", s1, other_core)
+    ed2 = send(name + "_ed2", d2, from_core(0))
+    es2 = send(name + "_es2", s2, from_core(1))
+    ed3 = send(name + "_ed3", d3, end_core(0))
+    es3 = send(name + "_es3", s3, end_core(1))
+    return (near, far, d1, s1, ed1, es1), (d2, s2, ed2, es2), (d3, s3, ed3, es3)
+
+
+def turn_tables(positions):
+    cos_r, sin_r, cos_c, sin_c = rope_tables(positions, HD)
+    cosine = jnp.concatenate([cos_r, cos_r, cos_c, cos_c] * 2, 1)
+    sine = jnp.concatenate([-sin_r, sin_r, -sin_c, sin_c] * 2, 1)
+    return cosine, sine
+
+
+def ints(*values):
+    return jnp.stack([jnp.asarray(v, jnp.int32) for v in values])
+
+
+def local_lines(
+    tokens,
+    norm_gain,
+    query_weight,
+    key_weight,
+    value_weight,
+    pool_in_weight,
+    pool_mix_weight,
+    sink_logit,
+    out_pool_weight,
+    out_attn_weight,
+):
+    s, t = lax.axis_index("sp"), lax.axis_index("tp")
+    z, y, x, c = s // 2, s % 2, t // 2, t % 2
+    home = y == c
+    planes = lax.axis_size("sp") // 2
+    tok_rows = tokens.shape[0]
+    seq_total = tok_rows * lax.axis_size("sp")
+    offset = (2 * z + c) * tok_rows
+    group = 2 * x + y
+    outer = (z == 0) | (z == planes - 1)
+
+    w_in = pack("pack_in", (query_weight, key_weight, value_weight, pool_in_weight), 1)
+    in_swapped = send("in_swap", w_in, swap_away)
+    near = jnp.where(home, w_in, send("in_near", w_in, home_to_away))
+    far = jnp.where(home, send("in_far", in_swapped, away_to_home), in_swapped)
+    in_near, in_two, in_three = line_gather("in", near, far)
+
+    p1 = send("tok1", tokens, token_one)
+    p2 = send("tok2", tokens, token_two)
+    p3 = send("tok3", tokens, away_to_home)
+    p4 = send("tok4", p1, token_diag)
+    p5 = send("tok5", p2, token_diag)
+
+    w_out = pack("pack_out", (out_pool_weight, out_attn_weight), 0)
+    out_swapped = send("out_swap", w_out, swap_away)
+    mix_other = send("mix_swap", pool_mix_weight[0], swap_away)
+    sink_other = send("sink_swap", sink_logit, swap_away)
+    mix = jnp.where(home, pool_mix_weight[0], mix_other)
+    sink = jnp.where(home, sink_logit, sink_other)
+    o_near = jnp.where(home, w_out, send("out_near", w_out, home_to_away))
+    o_far = jnp.where(home, send("out_far", out_swapped, away_to_home), out_swapped)
+    out_near, out_two, out_three = line_gather("out", o_near, o_far)
+
+    zr = jnp.where(c == 0, z - 1, z + 1)
+    ze = jnp.where(c == 0, z + 1, z - 1)
+    z2 = jnp.where(z < planes // 2, z + 2, z - 2)
+    z3 = planes - 1 - z
+    has_r = (zr >= 0) & (zr < planes)
+    has_e = (ze >= 0) & (ze < planes)
+
+    head = ints(home, 2 * x + c, 2 * x + 1 - c, 2 * (1 - x) + c, 2 * (1 - x) + 1 - c)
+    normed = norm_tokens(head, (tokens, p1, p2, p3, p4, p5), norm_gain[None, :])
+
+    near_idx = ints(
+        2 * z + y,
+        2 * z + 1 - y,
+        jnp.where(has_r, 2 * zr + y, -1),
+        jnp.where(has_r, 2 * zr + 1 - y, -1),
+        jnp.where(has_e, 2 * ze + y, -1),
+        jnp.where(has_e, 2 * ze + 1 - y, -1),
+    )
+    acc = project_near(near_idx, normed, in_near)
+    far_idx = ints(c, 2 * z2 + y, 2 * z2 + 1 - y, 2 * z3 + y, 2 * z3 + 1 - y)
+    widths = (query_weight.shape[1], key_weight.shape[1])
+    tables = turn_tables(offset + jnp.arange(tok_rows, dtype=jnp.int32))
+    query, pair, pool_input, low, high = project_far(far_idx, normed, acc, tables, in_two + in_three, widths)
+
+    before = send("halo_next", high, halo_next)
+    behind = send("halo_prev", low, halo_prev)
+    place = ints(group, offset)
+    pool_out = pool_mixer(place, pool_input, before, behind, mix, seq_total)
+    attended, log_here = attend(place, query, pair, before, behind, sink, seq_total)
+    log_weight = jnp.where(home, log_here, send("log_swap", log_here, swap_away))
+
+    def slot(zz, parity, ok):
+        return jnp.where(ok, 2 * (zz ^ group) + parity, -1)
+
+    early_idx = ints(
+        c,
+        slot(z, y, True),
+        slot(z, 1 - y, True),
+        slot(zr, y, has_r),
+        slot(zr, 1 - y, has_r),
+        slot(ze, y, has_e),
+        slot(ze, 1 - y, has_e),
+        slot(z2, y, outer),
+        slot(z2, 1 - y, outer),
+    )
+    blocks = out_early(early_idx, pool_out, attended, out_near + out_two)
+    late = out_late(ints(c, outer, y, 1 - y), pool_out, attended, out_two + out_three)
+    early_parts = [send(f"early{r}", blocks[r], part_early(r)) for r in range(4)]
+    late_parts = [send(f"late{r}", late, part_late(r)) for r in range(4)]
+    last = jnp.where(z < planes // 2, planes - 1, 0)
+    mixed = sum_parts(ints(t == last, home, 0), early_parts, late_parts, blocks[0], late)
+    return (mixed, log_weight)
+
+
 def solution(mesh):
+    lines = mesh.shape["sp"] == 8 and mesh.shape["tp"] == 4
     return jax.shard_map(
-        local,
+        local_lines if lines else local,
         mesh=mesh,
         in_specs=(
             P("sp", "tp"),

time: 263 us -> 231 us (0.88)
  the two profiles are of different devices: /device:TPU:0 before, /device:TPU:24 now
where the time goes in v2:
time: 231 us; the launch traced here: 230 us
  starting transfers between devices  91.3 us (40%)
  Pallas kernels  71.1 us (31%)
  waiting for transfers between devices  50.8 us (22%)
  local copies, waits for them, and re-layouts  7.96 us (3%)
  other arithmetic  6.91 us (3%)
    ppermute x48, starting transfers between devices, send(): return lax.ppermute(value, ('sp', 'tp'), make_perm(rule))  91.3 us
    ppermute x48, waiting for transfers between devices, send(): return lax.ppermute(value, ('sp', 'tp'), make_perm(rule))  50.8 us
    pallas_call x2, Pallas kernels, pack(): pl.pallas_call(functools.partial(pack_kernel, axis), out_shape=jax.ShapeD...  30.1 us
    pallas_call x1, Pallas kernels, attend(): pl.pallas_call(functools.partial(attend_kernel, seq_total), out_shape=[ja...  8.48 us
    pallas_call x1, Pallas kernels, project_far(): pl.pallas_call(functools.partial(far_kernel, widths), out_shape=[jax.Shap...  6.37 us
    pallas_call x1, Pallas kernels, out_early(): pl.pallas_call(early_kernel, out_shape=[jax.ShapeDtypeStruct((rows, 2 * w...  5.98 us
    pallas_call x1, Pallas kernels, project_near(): pl.pallas_call(near_kernel, out_shape=jax.ShapeDtypeStruct((rows, cols),...  5.67 us
    pallas_call x1, Pallas kernels, norm_tokens(): pl.pallas_call(norm_kernel, out_shape=jax.ShapeDtypeStruct((8, rows, wide...  4.83 us
  transfers between devices with their start and end apart: 48, of which 9 were waited for; matrix products, arithmetic and copies ran while one was open for 5% of the time, Pallas kernels for 22%

profile of v2, /device:TPU:24, one launch (start us, length us, event | category | flops | bytes accessed | tf_op | source)
XLA Modules:
  0.0 230.1 jit_solution(2763019621219509493)
XLA Ops:
  0.6 17.0 %pack_in.1 = bf16[256,1024]{1,0:T(8,128)(2,1)} custom-call(bf16[256,512]{1,0:T(8,128)(2,1)} %refs_0_.2, bf16[256,128]{1,0:T(8,128)(2,1)} %refs_1_.2, bf16[256,128]{1,0:T(8,128)(2,1)} %refs_2_.1, bf16[256,256]{1,0:T(8,128)(2,1)} %refs_3_.1), custom_call_target="tpu_custom_call" | custom-call | tf_op jit(solution)/shard_map/pack_in/pallas_call | solution.py:338
  18.4 4.8 %collective-permute-start.5 = (bf16[256,1024]{1,0:T(8,128)(2,1)}, bf16[256,1024]{1,0:T(8,128)(2,1)S(1)}, u32[]{:S(2)}, u32[]{:S(2)}) collective-permute-start(bf16[256,1024]{1,0:T(8,128)(2,1)} %pack_in.1), channel_id=1, source_target_pairs={{0,1},{2,3},{5,4},{7,6},{8,9},{10,11},{13,12},{15,14},{16,17},{18,... | collective-permute-start | bytes 1572872 | tf_op jit(solution)/shard_map/in_near/ppermute | solution.py:221
  23.2 13.0 %pack_out.1 = bf16[768,256]{1,0:T(8,128)(2,1)} custom-call(bf16[256,256]{1,0:T(8,128)(2,1)} %refs_0_.3, bf16[512,256]{1,0:T(8,128)(2,1)} %refs_1_.3), custom_call_target="tpu_custom_call" | custom-call | tf_op jit(solution)/shard_map/pack_out/pallas_call | solution.py:338
  43.8 2.4 %collective-permute-start.1 = (bf16[512,512]{1,0:T(8,128)(2,1)S(1)}, bf16[512,512]{1,0:T(8,128)(2,1)S(1)}, u32[]{:S(2)}, u32[]{:S(2)}) collective-permute-start(bf16[512,512]{1,0:T(8,128)(2,1)S(1)} %copy-done.18), channel_id=1, source_target_pairs={{0,4},{1,2},{2,6},{3,0},{4,7},{5,1},{6,5},{7,3},{8,12},{9,10},{10,... | collective-permute-start | bytes 1572872 | tf_op jit(solution)/shard_map/tok2/ppermute | solution.py:221
  48.9 2.4 %collective-permute-done.8.d1 = bf16[256,1024]{1,0:T(8,128)(2,1)S(1)} collective-permute-done((bf16[256,1024]{1,0:T(8,128)(2,1)S(1)}, bf16[256,1024]{1,0:T(8,128)(2,1)S(1)}, u32[]{:S(2)}, u32[]{:S(2)}) %collective-permute-start.8) | collective-permute-done | bytes 524320 | tf_op jit(solution)/shard_map/in_d1/ppermute | solution.py:221
  55.8 2.8 %collective-permute-done.1.p2 = bf16[512,512]{1,0:T(8,128)(2,1)S(1)} collective-permute-done((bf16[512,512]{1,0:T(8,128)(2,1)S(1)}, bf16[512,512]{1,0:T(8,128)(2,1)S(1)}, u32[]{:S(2)}, u32[]{:S(2)}) %collective-permute-start.1) | collective-permute-done | bytes 524320 | tf_op jit(solution)/shard_map/tok2/ppermute | solution.py:221
  61.3 4.5 %collective-permute-done.26 = bf16[768,256]{1,0:T(8,128)(2,1)S(1)} collective-permute-done((bf16[768,256]{1,0:T(8,128)(2,1)S(1)}, bf16[768,256]{1,0:T(8,128)(2,1)S(1)}, u32[]{:S(2)}, u32[]{:S(2)}) %collective-permute-start.26) | collective-permute-done | bytes 393248 | tf_op jit(solution)/shard_map/out_far/ppermute | solution.py:221
  66.5 2.1 collective-permute-done.27.refs_2_
  68.6 5.6 %collective-permute-start.10 = (bf16[256,1024]{1,0:T(8,128)(2,1)S(1)}, bf16[256,1024]{1,0:T(8,128)(2,1)S(1)}, u32[]{:S(2)}, u32[]{:S(2)}) collective-permute-start(bf16[256,1024]{1,0:T(8,128)(2,1)S(1)} %collective-permute-done.8.d1), channel_id=1, source_target_pairs={{0,1},{1,0},{2,3},{3,2},{4,5},{5,4},{6,7},{7,6},{8,9},{9,8},{10,11... | collective-permute-start | bytes 1572872 | tf_op jit(solution)/shard_map/in_ed1/ppermute | solution.py:221
  79.1 4.2 %collective-permute-start.11 = (bf16[256,1024]{1,0:T(8,128)(2,1)}, bf16[256,1024]{1,0:T(8,128)(2,1)}, u32[]{:S(2)}, u32[]{:S(2)}) collective-permute-start(bf16[256,1024]{1,0:T(8,128)(2,1)} %collective-permute-done.9.s1), channel_id=1, source_target_pairs={{0,1},{1,0},{2,3},{3,2},{4,5},{5,4},{6,7},{7,6},{8,9},{9,8},{10,11... | collective-permute-start | bytes 1572872 | tf_op jit(solution)/shard_map/in_es1/ppermute | solution.py:221
  83.3 13.7 %collective-permute-done.28.refs_3_ = bf16[768,256]{1,0:T(8,128)(2,1)} collective-permute-done((bf16[768,256]{1,0:T(8,128)(2,1)S(1)}, bf16[768,256]{1,0:T(8,128)(2,1)}, u32[]{:S(2)}, u32[]{:S(2)}) %collective-permute-start.28) | collective-permute-done | bytes 393248 | tf_op jit(solution)/shard_map/out_s1/ppermute | solution.py:221
  97.0 2.1 collective-permute-start.14
  100.4 4.6 %collective-permute-start.18 = (bf16[256,1024]{1,0:T(8,128)(2,1)S(1)}, bf16[256,1024]{1,0:T(8,128)(2,1)}, u32[]{:S(2)}, u32[]{:S(2)}) collective-permute-start(bf16[256,1024]{1,0:T(8,128)(2,1)S(1)} %collective-permute-done.16.refs_4_), channel_id=1, source_target_pairs={{0,1},{2,3},{4,5},{6,7},{24,25},{26,27},{28,29},{30,31}} | collective-permute-start | bytes 1572872 | tf_op jit(solution)/shard_map/in_ed3/ppermute | solution.py:221
  106.4 2.0 collective-permute-start.29
  111.7 1.9 multiply_sine_fusion
  119.1 4.8 %norm.1.normed = bf16[8,512,256]{2,1,0:T(8,128)(2,1)} custom-call(s32[5]{0:T(128)} %stack.150.idx, bf16[512,512]{1,0:T(8,128)(2,1)} %own.1, bf16[512,512]{1,0:T(8,128)(2,1)} %copy-done.20, bf16[512,512]{1,0:T(8,128)(2,1)} %copy-done.21, bf16[512,512]{1,0:T(8,128)(2,1)} %copy-done.22, bf16[512,512]{1,0:T(8,128)(2,1)} %copy-done.23, ...), custom_call_target="tpu_custom_call" | custom-call | tf_op jit(solution)/shard_map/norm/pallas_call | solution.py:394
  124.0 5.7 %project_near.1.acc = f32[512,1024]{1,0:T(8,128)} custom-call(s32[6]{0:T(128)} %stack.157.idx, bf16[8,512,256]{2,1,0:T(8,128)(2,1)} %norm.1.normed, bf16[256,1024]{1,0:T(8,128)(2,1)} %copy-done, bf16[256,1024]{1,0:T(8,128)(2,1)} %copy-done.1, bf16[256,1024]{1,0:T(8,128)(2,1)} %copy-done.19, bf16[256,1024]{1,0:T(8,128)(2,1)} %collective-permute-done.9.s1, ...), custom_call_target="tpu_custom_call" | custom-call | tf_op jit(solution)/shard_map/project_near/pallas_call | solution.py:431
  130.4 6.4 %project_far.1 = (bf16[512,512]{1,0:T(8,128)(2,1)}, bf16[512,256]{1,0:T(8,128)(2,1)}, bf16[512,256]{1,0:T(8,128)(2,1)}, bf16[136,256]{1,0:T(8,128)(2,1)}, bf16[136,256]{1,0:T(8,128)(2,1)}) custom-call(s32[5]{0:T(128)} %stack.145.idx, bf16[8,512,256]{2,1,0:T(8,128)(2,1)} %norm.1.normed, f32[512,1024]{1,0:T(8,128)} %project_near.1.acc, ...), custom_call_target="tpu_custom_call" | custom-call | tf_op jit(solution)/shard_map/project_far/pallas_call | solution.py:486
  136.7 5.6 %collective-permute-start.20 = (bf16[136,256]{1,0:T(8,128)(2,1)}, bf16[136,256]{1,0:T(8,128)(2,1)S(1)}, u32[]{:S(2)}, u32[]{:S(2)}) collective-permute-start(bf16[136,256]{1,0:T(8,128)(2,1)} %get-tuple-element.14), channel_id=1, source_target_pairs={{0,1},{1,8},{2,3},{3,10},{4,5},{5,12},{6,7},{7,14},{8,9},{9,16},{1... | collective-permute-start | bytes 208904 | tf_op jit(solution)/shard_map/halo_next/ppermute | solution.py:221
  142.3 3.3 %collective-permute-start.21 = (bf16[136,256]{1,0:T(8,128)(2,1)}, bf16[136,256]{1,0:T(8,128)(2,1)S(1)}, u32[]{:S(2)}, u32[]{:S(2)}) collective-permute-start(bf16[136,256]{1,0:T(8,128)(2,1)} %get-tuple-element.15), channel_id=1, source_target_pairs={{1,0},{3,2},{5,4},{7,6},{8,1},{9,8},{10,3},{11,10},{12,5},{13,12},... | collective-permute-start | bytes 208904 | tf_op jit(solution)/shard_map/halo_prev/ppermute | solution.py:221
  146.3 2.4 %collective-permute-start.33 = (bf16[768,256]{1,0:T(8,128)(2,1)S(1)}, bf16[768,256]{1,0:T(8,128)(2,1)S(1)}, u32[]{:S(2)}, u32[]{:S(2)}) collective-permute-start(bf16[768,256]{1,0:T(8,128)(2,1)S(1)} %collective-permute-done.31.refs_6_.refs_0_), channel_id=1, source_target_pairs={{0,1},{2,3},{4,5},{6,7},{8,9},{10,11},{12,13},{14,15},{16,17},{18,... | collective-permute-start | bytes 1179656 | tf_op jit(solution)/shard_map/out_ed2/ppermute | solution.py:221
  153.4 2.4 %pool.1.pooled = bf16[512,256]{1,0:T(8,128)(2,1)} custom-call(s32[2]{0:T(128)} %pad_add_fusion.1.idx, bf16[512,256]{1,0:T(8,128)(2,1)} %get-tuple-element.13.own, bf16[136,256]{1,0:T(8,128)(2,1)} %copy-done.32, bf16[136,256]{1,0:T(8,128)(2,1)} %copy-done.33, bf16[256,256]{1,0:T(8,128)(2,1)} %broadcast_select_fusion.4.mix), custom_call_target="tpu_custom_call" | custom-call | tf_op jit(solution)/shard_map/pool/pallas_call | solution.py:522
  155.7 8.5 %attend.1 = (bf16[512,512]{1,0:T(8,128)(2,1)}, f32[8,512]{1,0:T(8,128)}) custom-call(s32[2]{0:T(128)} %pad_add_fusion.1.idx, bf16[512,512]{1,0:T(8,128)(2,1)} %get-tuple-element.16.query, bf16[512,256]{1,0:T(8,128)(2,1)} %get-tuple-element.17.pair, bf16[136,256]{1,0:T(8,128)(2,1)} %copy-done.32, bf16[136,256]{1,0:T(8,128)(2,1)} %copy-done.33, ...), custom_call_target="tpu_custom_call" | custom-call | tf_op jit(solution)/shard_map/attend/pallas_call | solution.py:591
  165.3 6.0 %out_early.1 = (bf16[512,512]{1,0:T(8,128)(2,1)}, bf16[512,512]{1,0:T(8,128)(2,1)}, bf16[512,512]{1,0:T(8,128)(2,1)}, bf16[512,512]{1,0:T(8,128)(2,1)}) custom-call(s32[9]{0:T(128)} %stack.137.idx, bf16[512,256]{1,0:T(8,128)(2,1)} %pool.1.pooled, bf16[512,512]{1,0:T(8,128)(2,1)} %get-tuple-element.18.attended, bf16[768,256]{1,0:T(8,128)(2,1)} %copy-done.6, ...), custom_call_target="tpu_custom_call" | custom-call | tf_op jit(solution)/shard_map/out_early/pallas_call | solution.py:633
  172.0 5.2 %collective-permute-start.36 = (bf16[512,512]{1,0:T(8,128)(2,1)}, bf16[512,512]{1,0:T(8,128)(2,1)S(1)}, u32[]{:S(2)}, u32[]{:S(2)}) collective-permute-start(bf16[512,512]{1,0:T(8,128)(2,1)} %get-tuple-element.20), channel_id=1, source_target_pairs={{0,1},{1,5},{4,0},{5,4},{6,2},{7,6},{8,9},{9,13},{12,8},{13,12},{1... | collective-permute-start | bytes 1572872 | tf_op jit(solution)/shard_map/early1/ppermute | solution.py:221
  177.2 4.3 %collective-permute-start.37 = (bf16[512,512]{1,0:T(8,128)(2,1)}, bf16[512,512]{1,0:T(8,128)(2,1)S(1)}, u32[]{:S(2)}, u32[]{:S(2)}) collective-permute-start(bf16[512,512]{1,0:T(8,128)(2,1)} %get-tuple-element.21), channel_id=1, source_target_pairs={{0,2},{1,6},{2,0},{3,4},{6,1},{7,5},{8,10},{9,14},{10,8},{11,12},{... | collective-permute-start | bytes 1572872 | tf_op jit(solution)/shard_map/early2/ppermute | solution.py:221
  181.5 3.1 %collective-permute-start.41 = (bf16[768,256]{1,0:T(8,128)(2,1)S(1)}, bf16[768,256]{1,0:T(8,128)(2,1)S(1)}, u32[]{:S(2)}, u32[]{:S(2)}) collective-permute-start(bf16[768,256]{1,0:T(8,128)(2,1)S(1)} %collective-permute-done.39.refs_4_), channel_id=1, source_target_pairs={{0,1},{2,3},{4,5},{6,7},{24,25},{26,27},{28,29},{30,31}} | collective-permute-start | bytes 1179656 | tf_op jit(solution)/shard_map/out_ed3/ppermute | solution.py:221
  189.0 4.0 %out_late.1.refs_9_ = bf16[512,512]{1,0:T(8,128)(2,1)} custom-call(s32[4]{0:T(128)} %pad_add_fusion.2.idx, bf16[512,256]{1,0:T(8,128)(2,1)} %pool.1.pooled, bf16[512,512]{1,0:T(8,128)(2,1)} %get-tuple-element.18.attended, bf16[768,256]{1,0:T(8,128)(2,1)} %copy-done.2, bf16[768,256]{1,0:T(8,128)(2,1)} %copy-done.3, bf16[768,256]{1,0:T(8,128)(2,1)} %copy-done.4, ...), custom_call_target="tpu_custom_call" | custom-call | tf_op jit(solution)/shard_map/out_late/pallas_call | solution.py:670
  195.1 5.1 %collective-permute-start.38 = (bf16[512,512]{1,0:T(8,128)(2,1)}, bf16[512,512]{1,0:T(8,128)(2,1)S(1)}, u32[]{:S(2)}, u32[]{:S(2)}) collective-permute-start(bf16[512,512]{1,0:T(8,128)(2,1)} %get-tuple-element.22), channel_id=1, source_target_pairs={{2,1},{3,5},{4,2},{5,6},{6,0},{7,4},{10,9},{11,13},{12,10},{13,14}... | collective-permute-start | bytes 1572872 | tf_op jit(solution)/shard_map/early3/ppermute | solution.py:221
  204.1 8.6 %collective-permute-done.38.refs_3_ = bf16[512,512]{1,0:T(8,128)(2,1)S(1)} collective-permute-done((bf16[512,512]{1,0:T(8,128)(2,1)}, bf16[512,512]{1,0:T(8,128)(2,1)S(1)}, u32[]{:S(2)}, u32[]{:S(2)}) %collective-permute-start.38) | collective-permute-done | bytes 524320 | tf_op jit(solution)/shard_map/early3/ppermute | solution.py:221
  212.8 13.8 %collective-permute-done.45.refs_6_ = bf16[512,512]{1,0:T(8,128)(2,1)} collective-permute-done((bf16[512,512]{1,0:T(8,128)(2,1)}, bf16[512,512]{1,0:T(8,128)(2,1)}, u32[]{:S(2)}, u32[]{:S(2)}) %collective-permute-start.45) | collective-permute-done | bytes 524320 | tf_op jit(solution)/shard_map/late2/ppermute | solution.py:221
  226.6 3.3 %sum.1 = bf16[512,512]{1,0:T(8,128)(2,1)} custom-call(s32[3]{0:T(128)} %pad_add_fusion.idx, bf16[512,512]{1,0:T(8,128)(2,1)} %copy-done.12, bf16[512,512]{1,0:T(8,128)(2,1)} %copy-done.13, bf16[512,512]{1,0:T(8,128)(2,1)} %copy-done.14, bf16[512,512]{1,0:T(8,128)(2,1)} %copy-done.17, bf16[512,512]{1,0:T(8,128)(2,1)} %copy-done.15, ...), custom_call_target="tpu_custom_call" | custom-call | tf_op jit(solution)/shard_map/sum/pallas_call | solution.py:705
  (167 shorter events, 52.5 us)
Async XLA Ops:
  17.7 20.0 %collective-permute-start.6 = (bf16[256,1024]{1,0:T(8,128)(2,1)}, bf16[256,1024]{1,0:T(8,128)(2,1)S(1)}, u32[]{:S(2)}, u32[]{:S(2)}) collective-permute-start(bf16[256,1024]{1,0:T(8,128)(2,1)} %pack_in.1), channel_id=1, source_target_pairs={{1,4},{3,6},{4,1},{6,3},{9,12},{11,14},{12,9},{14,11},{17,20},{19,... | collective-permute-start | bytes 1572872 | tf_op jit(solution)/shard_map/in_swap/ppermute | solution.py:221
  18.4 20.6 %collective-permute-start.5 = (bf16[256,1024]{1,0:T(8,128)(2,1)}, bf16[256,1024]{1,0:T(8,128)(2,1)S(1)}, u32[]{:S(2)}, u32[]{:S(2)}) collective-permute-start(bf16[256,1024]{1,0:T(8,128)(2,1)} %pack_in.1), channel_id=1, source_target_pairs={{0,1},{2,3},{5,4},{7,6},{8,9},{10,11},{13,12},{15,14},{16,17},{18,... | collective-permute-start | bytes 1572872 | tf_op jit(solution)/shard_map/in_near/ppermute | solution.py:221
  43.8 14.7 %collective-permute-start.1 = (bf16[512,512]{1,0:T(8,128)(2,1)S(1)}, bf16[512,512]{1,0:T(8,128)(2,1)S(1)}, u32[]{:S(2)}, u32[]{:S(2)}) collective-permute-start(bf16[512,512]{1,0:T(8,128)(2,1)S(1)} %copy-done.18), channel_id=1, source_target_pairs={{0,4},{1,2},{2,6},{3,0},{4,7},{5,1},{6,5},{7,3},{8,12},{9,10},{10,... | collective-permute-start | bytes 1572872 | tf_op jit(solution)/shard_map/tok2/ppermute | solution.py:221
  46.2 13.6 %collective-permute-start.2 = (bf16[512,512]{1,0:T(8,128)(2,1)S(1)}, bf16[512,512]{1,0:T(8,128)(2,1)S(1)}, u32[]{:S(2)}, u32[]{:S(2)}) collective-permute-start(bf16[512,512]{1,0:T(8,128)(2,1)S(1)} %copy-done.18), channel_id=1, source_target_pairs={{1,0},{3,2},{4,5},{6,7},{9,8},{11,10},{12,13},{14,15},{17,16},{19,... | collective-permute-start | bytes 1572872 | tf_op jit(solution)/shard_map/tok3/ppermute | solution.py:221
  51.4 22.8 %collective-permute-start.12 = (bf16[256,1024]{1,0:T(8,128)(2,1)S(1)}, bf16[256,1024]{1,0:T(8,128)(2,1)S(1)}, u32[]{:S(2)}, u32[]{:S(2)}) collective-permute-start(bf16[256,1024]{1,0:T(8,128)(2,1)S(1)} %collective-permute-done.8.d1), channel_id=1, source_target_pairs={{8,16},{9,0},{10,18},{11,2},{12,20},{13,4},{14,22},{15,6},{16,24},... | collective-permute-start | bytes 1572872 | tf_op jit(solution)/shard_map/in_d2/ppermute | solution.py:221
  59.9 15.7 %collective-permute-start.3 = (bf16[512,512]{1,0:T(8,128)(2,1)S(1)}, bf16[512,512]{1,0:T(8,128)(2,1)S(1)}, u32[]{:S(2)}, u32[]{:S(2)}) collective-permute-start(bf16[512,512]{1,0:T(8,128)(2,1)S(1)} %collective-permute-done.p1), channel_id=1, source_target_pairs={{1,3},{3,1},{4,6},{6,4},{9,11},{11,9},{12,14},{14,12},{17,19},{19,... | collective-permute-start | bytes 1572872 | tf_op jit(solution)/shard_map/tok4/ppermute | solution.py:221
  60.6 17.0 %collective-permute-start.13 = (bf16[256,1024]{1,0:T(8,128)(2,1)}, bf16[256,1024]{1,0:T(8,128)(2,1)S(1)}, u32[]{:S(2)}, u32[]{:S(2)}) collective-permute-start(bf16[256,1024]{1,0:T(8,128)(2,1)} %collective-permute-done.9.s1), channel_id=1, source_target_pairs={{8,17},{9,1},{10,19},{11,3},{12,21},{13,5},{14,23},{15,7},{16,25},... | collective-permute-start | bytes 1572872 | tf_op jit(solution)/shard_map/in_s2/ppermute | solution.py:221
  65.8 13.3 %collective-permute-start.4 = (bf16[512,512]{1,0:T(8,128)(2,1)S(1)}, bf16[512,512]{1,0:T(8,128)(2,1)S(1)}, u32[]{:S(2)}, u32[]{:S(2)}) collective-permute-start(bf16[512,512]{1,0:T(8,128)(2,1)S(1)} %collective-permute-done.1.p2), channel_id=1, source_target_pairs={{1,3},{3,1},{4,6},{6,4},{9,11},{11,9},{12,14},{14,12},{17,19},{19,... | collective-permute-start | bytes 1572872 | tf_op jit(solution)/shard_map/tok5/ppermute | solution.py:221
  68.6 30.5 %collective-permute-start.10 = (bf16[256,1024]{1,0:T(8,128)(2,1)S(1)}, bf16[256,1024]{1,0:T(8,128)(2,1)S(1)}, u32[]{:S(2)}, u32[]{:S(2)}) collective-permute-start(bf16[256,1024]{1,0:T(8,128)(2,1)S(1)} %collective-permute-done.8.d1), channel_id=1, source_target_pairs={{0,1},{1,0},{2,3},{3,2},{4,5},{5,4},{6,7},{7,6},{8,9},{9,8},{10,11... | collective-permute-start | bytes 1572872 | tf_op jit(solution)/shard_map/in_ed1/ppermute | solution.py:221
  74.2 26.2 %collective-permute-start.16 = (bf16[256,1024]{1,0:T(8,128)(2,1)S(1)}, bf16[256,1024]{1,0:T(8,128)(2,1)S(1)}, u32[]{:S(2)}, u32[]{:S(2)}) collective-permute-start(bf16[256,1024]{1,0:T(8,128)(2,1)S(1)} %collective-permute-done.12.refs_0_), channel_id=1, source_target_pairs={{8,0},{10,2},{12,4},{14,6},{16,24},{18,26},{20,28},{22,30}} | collective-permute-start | bytes 1572872 | tf_op jit(solution)/shard_map/in_d3/ppermute | solution.py:221
  76.3 20.7 %collective-permute-start.28 = (bf16[768,256]{1,0:T(8,128)(2,1)S(1)}, bf16[768,256]{1,0:T(8,128)(2,1)}, u32[]{:S(2)}, u32[]{:S(2)}) collective-permute-start(bf16[768,256]{1,0:T(8,128)(2,1)S(1)} %broadcast_select_fusion.2.refs_1_), channel_id=1, source_target_pairs={{0,8},{2,10},{4,12},{6,14},{8,16},{9,1},{10,18},{11,3},{12,20},{13... | collective-permute-start | bytes 1179656 | tf_op jit(solution)/shard_map/out_s1/ppermute | solution.py:221
  77.6 27.4 %collective-permute-start.17 = (bf16[256,1024]{1,0:T(8,128)(2,1)S(1)}, bf16[256,1024]{1,0:T(8,128)(2,1)}, u32[]{:S(2)}, u32[]{:S(2)}) collective-permute-start(bf16[256,1024]{1,0:T(8,128)(2,1)S(1)} %collective-permute-done.13.refs_1_), channel_id=1, source_target_pairs={{9,1},{11,3},{13,5},{15,7},{17,25},{19,27},{21,29},{23,31}} | collective-permute-start | bytes 1572872 | tf_op jit(solution)/shard_map/in_s3/ppermute | solution.py:221
  79.1 27.3 %collective-permute-start.11 = (bf16[256,1024]{1,0:T(8,128)(2,1)}, bf16[256,1024]{1,0:T(8,128)(2,1)}, u32[]{:S(2)}, u32[]{:S(2)}) collective-permute-start(bf16[256,1024]{1,0:T(8,128)(2,1)} %collective-permute-done.9.s1), channel_id=1, source_target_pairs={{0,1},{1,0},{2,3},{3,2},{4,5},{5,4},{6,7},{7,6},{8,9},{9,8},{10,11... | collective-permute-start | bytes 1572872 | tf_op jit(solution)/shard_map/in_es1/ppermute | solution.py:221
  105.1 24.6 %collective-permute-start.19 = (bf16[256,1024]{1,0:T(8,128)(2,1)}, bf16[256,1024]{1,0:T(8,128)(2,1)}, u32[]{:S(2)}, u32[]{:S(2)}) collective-permute-start(bf16[256,1024]{1,0:T(8,128)(2,1)} %collective-permute-done.17.refs_5_), channel_id=1, source_target_pairs={{1,0},{3,2},{5,4},{7,6},{25,24},{27,26},{29,28},{31,30}} | collective-permute-start | bytes 1572872 | tf_op jit(solution)/shard_map/in_es3/ppermute | solution.py:221
  106.4 39.9 %collective-permute-start.29 = (bf16[768,256]{1,0:T(8,128)(2,1)}, bf16[768,256]{1,0:T(8,128)(2,1)}, u32[]{:S(2)}, u32[]{:S(2)}) collective-permute-start(bf16[768,256]{1,0:T(8,128)(2,1)} %collective-permute-done.27.refs_2_), channel_id=1, source_target_pairs={{0,1},{1,0},{2,3},{3,2},{4,5},{5,4},{6,7},{7,6},{8,9},{9,8},{10,11... | collective-permute-start | bytes 1179656 | tf_op jit(solution)/shard_map/out_ed1/ppermute | solution.py:221
  108.4 37.9 %collective-permute-start.31 = (bf16[768,256]{1,0:T(8,128)(2,1)}, bf16[768,256]{1,0:T(8,128)(2,1)S(1)}, u32[]{:S(2)}, u32[]{:S(2)}) collective-permute-start(bf16[768,256]{1,0:T(8,128)(2,1)} %collective-permute-done.27.refs_2_), channel_id=1, source_target_pairs={{8,16},{9,0},{10,18},{11,2},{12,20},{13,4},{14,22},{15,6},{16,24},... | collective-permute-start | bytes 1179656 | tf_op jit(solution)/shard_map/out_d2/ppermute | solution.py:221
  109.7 39.1 %collective-permute-start.32 = (bf16[768,256]{1,0:T(8,128)(2,1)}, bf16[768,256]{1,0:T(8,128)(2,1)S(1)}, u32[]{:S(2)}, u32[]{:S(2)}) collective-permute-start(bf16[768,256]{1,0:T(8,128)(2,1)} %collective-permute-done.28.refs_3_), channel_id=1, source_target_pairs={{8,17},{9,1},{10,19},{11,3},{12,21},{13,5},{14,23},{15,7},{16,25},... | collective-permute-start | bytes 1179656 | tf_op jit(solution)/shard_map/out_s2/ppermute | solution.py:221
  110.4 31.9 %collective-permute-start.22 = (bf16[256,256]{1,0:T(8,128)(2,1)S(1)}, bf16[256,256]{1,0:T(8,128)(2,1)}, u32[]{:S(2)}, u32[]{:S(2)}) collective-permute-start(bf16[256,256]{1,0:T(8,128)(2,1)S(1)} %bitcast.33), channel_id=1, source_target_pairs={{1,4},{3,6},{4,1},{6,3},{9,12},{11,14},{12,9},{14,11},{17,20},{19,... | collective-permute-start | bytes 393224 | tf_op jit(solution)/shard_map/mix_swap/ppermute | solution.py:221
  136.7 13.3 %collective-permute-start.20 = (bf16[136,256]{1,0:T(8,128)(2,1)}, bf16[136,256]{1,0:T(8,128)(2,1)S(1)}, u32[]{:S(2)}, u32[]{:S(2)}) collective-permute-start(bf16[136,256]{1,0:T(8,128)(2,1)} %get-tuple-element.14), channel_id=1, source_target_pairs={{0,1},{1,8},{2,3},{3,10},{4,5},{5,12},{6,7},{7,14},{8,9},{9,16},{1... | collective-permute-start | bytes 208904 | tf_op jit(solution)/shard_map/halo_next/ppermute | solution.py:221
  146.3 17.9 %collective-permute-start.30 = (bf16[768,256]{1,0:T(8,128)(2,1)}, bf16[768,256]{1,0:T(8,128)(2,1)S(1)}, u32[]{:S(2)}, u32[]{:S(2)}) collective-permute-start(bf16[768,256]{1,0:T(8,128)(2,1)} %collective-permute-done.28.refs_3_), channel_id=1, source_target_pairs={{0,1},{1,0},{2,3},{3,2},{4,5},{5,4},{6,7},{7,6},{8,9},{9,8},{10,11... | collective-permute-start | bytes 1179656 | tf_op jit(solution)/shard_map/out_es1/ppermute | solution.py:221
  146.3 17.9 %collective-permute-start.33 = (bf16[768,256]{1,0:T(8,128)(2,1)S(1)}, bf16[768,256]{1,0:T(8,128)(2,1)S(1)}, u32[]{:S(2)}, u32[]{:S(2)}) collective-permute-start(bf16[768,256]{1,0:T(8,128)(2,1)S(1)} %collective-permute-done.31.refs_6_.refs_0_), channel_id=1, source_target_pairs={{0,1},{2,3},{4,5},{6,7},{8,9},{10,11},{12,13},{14,15},{16,17},{18,... | collective-permute-start | bytes 1179656 | tf_op jit(solution)/shard_map/out_ed2/ppermute | solution.py:221
  148.8 32.7 %collective-permute-start.39 = (bf16[768,256]{1,0:T(8,128)(2,1)S(1)}, bf16[768,256]{1,0:T(8,128)(2,1)S(1)}, u32[]{:S(2)}, u32[]{:S(2)}) collective-permute-start(bf16[768,256]{1,0:T(8,128)(2,1)S(1)} %collective-permute-done.31.refs_6_.refs_0_), channel_id=1, source_target_pairs={{8,0},{10,2},{12,4},{14,6},{16,24},{18,26},{20,28},{22,30}} | collective-permute-start | bytes 1179656 | tf_op jit(solution)/shard_map/out_d3/ppermute | solution.py:221
  150.1 14.2 %collective-permute-start.34 = (bf16[768,256]{1,0:T(8,128)(2,1)S(1)}, bf16[768,256]{1,0:T(8,128)(2,1)S(1)}, u32[]{:S(2)}, u32[]{:S(2)}) collective-permute-start(bf16[768,256]{1,0:T(8,128)(2,1)S(1)} %collective-permute-done.32.refs_7_.refs_1_), channel_id=1, source_target_pairs={{1,0},{3,2},{5,4},{7,6},{9,8},{11,10},{13,12},{15,14},{17,16},{19,... | collective-permute-start | bytes 1179656 | tf_op jit(solution)/shard_map/out_es2/ppermute | solution.py:221
  151.4 33.2 %collective-permute-start.40 = (bf16[768,256]{1,0:T(8,128)(2,1)S(1)}, bf16[768,256]{1,0:T(8,128)(2,1)S(1)}, u32[]{:S(2)}, u32[]{:S(2)}) collective-permute-start(bf16[768,256]{1,0:T(8,128)(2,1)S(1)} %collective-permute-done.32.refs_7_.refs_1_), channel_id=1, source_target_pairs={{9,1},{11,3},{13,5},{15,7},{17,25},{19,27},{21,29},{23,31}} | collective-permute-start | bytes 1179656 | tf_op jit(solution)/shard_map/out_s3/ppermute | solution.py:221
  171.3 23.8 %collective-permute-start.35 = (bf16[512,512]{1,0:T(8,128)(2,1)}, bf16[512,512]{1,0:T(8,128)(2,1)S(1)}, u32[]{:S(2)}, u32[]{:S(2)}) collective-permute-start(bf16[512,512]{1,0:T(8,128)(2,1)} %get-tuple-element.19.refs_8_), channel_id=1, source_target_pairs={{1,4},{3,6},{4,1},{9,12},{11,14},{12,9},{19,22},{20,17},{22,19},{2... | collective-permute-start | bytes 1572872 | tf_op jit(solution)/shard_map/early0/ppermute | solution.py:221
  172.0 28.2 %collective-permute-start.36 = (bf16[512,512]{1,0:T(8,128)(2,1)}, bf16[512,512]{1,0:T(8,128)(2,1)S(1)}, u32[]{:S(2)}, u32[]{:S(2)}) collective-permute-start(bf16[512,512]{1,0:T(8,128)(2,1)} %get-tuple-element.20), channel_id=1, source_target_pairs={{0,1},{1,5},{4,0},{5,4},{6,2},{7,6},{8,9},{9,13},{12,8},{13,12},{1... | collective-permute-start | bytes 1572872 | tf_op jit(solution)/shard_map/early1/ppermute | solution.py:221
  177.2 24.4 %collective-permute-start.37 = (bf16[512,512]{1,0:T(8,128)(2,1)}, bf16[512,512]{1,0:T(8,128)(2,1)S(1)}, u32[]{:S(2)}, u32[]{:S(2)}) collective-permute-start(bf16[512,512]{1,0:T(8,128)(2,1)} %get-tuple-element.21), channel_id=1, source_target_pairs={{0,2},{1,6},{2,0},{3,4},{6,1},{7,5},{8,10},{9,14},{10,8},{11,12},{... | collective-permute-start | bytes 1572872 | tf_op jit(solution)/shard_map/early2/ppermute | solution.py:221
  193.1 19.7 %collective-permute-start.43 = (bf16[512,512]{1,0:T(8,128)(2,1)}, bf16[512,512]{1,0:T(8,128)(2,1)S(1)}, u32[]{:S(2)}, u32[]{:S(2)}) collective-permute-start(bf16[512,512]{1,0:T(8,128)(2,1)} %out_late.1.refs_9_), channel_id=1, source_target_pairs={{6,3},{14,11},{17,20},{25,28}} | collective-permute-start | bytes 1572872 | tf_op jit(solution)/shard_map/late0/ppermute | solution.py:221
  193.8 19.0 %collective-permute-start.44 = (bf16[512,512]{1,0:T(8,128)(2,1)}, bf16[512,512]{1,0:T(8,128)(2,1)S(1)}, u32[]{:S(2)}, u32[]{:S(2)}) collective-permute-start(bf16[512,512]{1,0:T(8,128)(2,1)} %out_late.1.refs_9_), channel_id=1, source_target_pairs={{2,3},{3,7},{10,11},{11,15},{20,16},{21,20},{28,24},{29,28}} | collective-permute-start | bytes 1572872 | tf_op jit(solution)/shard_map/late1/ppermute | solution.py:221
  195.1 17.6 %collective-permute-start.38 = (bf16[512,512]{1,0:T(8,128)(2,1)}, bf16[512,512]{1,0:T(8,128)(2,1)S(1)}, u32[]{:S(2)}, u32[]{:S(2)}) collective-permute-start(bf16[512,512]{1,0:T(8,128)(2,1)} %get-tuple-element.22), channel_id=1, source_target_pairs={{2,1},{3,5},{4,2},{5,6},{6,0},{7,4},{10,9},{11,13},{12,10},{13,14}... | collective-permute-start | bytes 1572872 | tf_op jit(solution)/shard_map/early3/ppermute | solution.py:221
  200.2 26.3 %collective-permute-start.45 = (bf16[512,512]{1,0:T(8,128)(2,1)}, bf16[512,512]{1,0:T(8,128)(2,1)}, u32[]{:S(2)}, u32[]{:S(2)}) collective-permute-start(bf16[512,512]{1,0:T(8,128)(2,1)} %out_late.1.refs_9_), channel_id=1, source_target_pairs={{4,3},{5,7},{12,11},{13,15},{18,16},{19,20},{26,24},{27,28}} | collective-permute-start | bytes 1572872 | tf_op jit(solution)/shard_map/late2/ppermute | solution.py:221
  201.6 25.0 %collective-permute-start.46 = (bf16[512,512]{1,0:T(8,128)(2,1)}, bf16[512,512]{1,0:T(8,128)(2,1)}, u32[]{:S(2)}, u32[]{:S(2)}) collective-permute-start(bf16[512,512]{1,0:T(8,128)(2,1)} %out_late.1.refs_9_), channel_id=1, source_target_pairs={{0,3},{1,7},{8,11},{9,15},{22,16},{23,20},{30,24},{31,28}} | collective-permute-start | bytes 1572872 | tf_op jit(solution)/shard_map/late3/ppermute | solution.py:221
  (53 other events, 974.8 us)
